TPU v7x, 32 devices: a whole 2x2x4 slice. The times are simulated.
32 devices in a mesh: rep: 2 (over y), fs: 4 (over z), tp: 4 (over x, core).
Axes of the slice: x: 2, y: 2, z: 4, core: 2. Of those that a mesh axis runs over, the one named last changes fastest.
Arguments:
- tokens: bfloat16 [4096, 2048], P(('rep', 'fs'), 'tp'), may hold values from -6 to 6
- pre_gain: float32 [2048], replicated, may hold values from 0.1 to 1.9
- u_weight: float32 [2048, 512], P('fs', 'tp'), may hold values from -0.125 to 0.125
- u_scale: float32 [512], P('tp'), may hold values from 0.5 to 2
- v_weight: float32 [2048, 512], P('fs', 'tp'), may hold values from -0.125 to 0.125
- v_scale: float32 [512], P('tp'), may hold values from 0.5 to 2
- group_gain: float32 [512], P('tp'), may hold values from 0.1 to 1.9
- span_weight: bfloat16 [8, 128, 128], P('tp'), may hold values from -0.5 to 0.5
- span_bias: float32 [8, 128], P('tp'), may hold values from 0.5 to 1.5
- out_weight: float32 [512, 2048], P('tp', 'fs'), may hold values from -0.25 to 0.25
- out_scale: float32 [2048], P('fs'), may hold values from 0.5 to 2
- ffn_gain: float32 [2048], replicated, may hold values from 0.1 to 1.9
- gate_weight: float32 [2048, 5632], P('fs', 'tp'), may hold values from -0.125 to 0.125
- gate_scale: float32 [5632], P('tp'), may hold values from 0.5 to 2
- up_weight: float32 [2048, 5632], P('fs', 'tp'), may hold values from -0.125 to 0.125
- up_scale: float32 [5632], P('tp'), may hold values from 0.5 to 2
- down_weight: float32 [5632, 2048], P('tp', 'fs'), may hold values from -0.078125 to 0.078125
- down_scale: float32 [2048], P('fs'), may hold values from 0.5 to 2
Outputs:
- layer_out: bfloat16 [4096, 2048], P(('rep', 'fs'), 'tp')
All inputs are finite; a program needn't handle non-finite values.
Results may differ from a plain program's by a relative error of at most 0.02.
Values may be sent and summed in bfloat16 or wider, within the bound.
A program may use at most 64 MiB of HBM per device.

v0:
```python
import functools

import jax
import jax.numpy as jnp
from jax import lax
from jax.experimental import pallas as pl
from jax.experimental.pallas import tpu as pltpu
from jax.sharding import PartitionSpec as P

EPS = 0.02
MESH = pl.DeviceIdType.MESH
SCALES, MIXER_IN, MIXER_OUT, GATE, UP, DOWN_A, DOWN_B = range(7)
KINDS = 7
TOKENS, OUT_ROWS, GATED = range(3)


def layer_kernel(
    sizes,
    tokens_ref,
    scales_ref,
    uv_ref,
    out_ref,
    gate_ref,
    up_ref,
    down_ref,
    pre_gain_ref,
    ffn_gain_ref,
    u_scale_ref,
    v_scale_ref,
    group_gain_ref,
    lower_ref,
    bias_ref,
    gate_scale_ref,
    up_scale_ref,
    result_ref,
    tok_all,
    scale_all,
    uv_all,
    out_all,
    gate_all,
    up_all,
    down_all,
    normed,
    gated_all,
    gate_acc,
    up_acc,
    hidden,
    ffn_acc,
    part,
    parts_in,
    local_sem,
    ring_send,
    ring_recv,
    tp_send,
    tp_recv,
    part_send,
    part_recv,
):
    n_rep, n_fs, n_tp = sizes
    n_ring = n_rep * n_fs
    far, near = n_ring // 2, n_ring - 1 - n_ring // 2
    hops = {SCALES: (far, near), MIXER_IN: (far, near), MIXER_OUT: (near, far), GATE: (far, near),
            UP: (near, far), DOWN_A: (far, near), DOWN_B: (near, far)}
    rows, own_width = tokens_ref.shape
    block = normed.shape[2]
    per_own = own_width // block
    rep, fs, tp = lax.axis_index("rep"), lax.axis_index("fs"), lax.axis_index("tp")

    def place(r, f):
        return r * n_fs + jnp.where(lax.rem(r, 2) == 0, f, n_fs - 1 - f)

    def coords(q):
        r, f = q // n_fs, lax.rem(q, n_fs)
        return r, jnp.where(lax.rem(r, 2) == 0, f, n_fs - 1 - f)

    me = place(rep, fs)

    def at_hop(way, hop):
        return lax.rem(me - hop + n_ring, n_ring) if way == 0 else lax.rem(me + hop, n_ring)

    def ring_id(way):
        r, f = coords(at_hop(1 - way, 1))
        return {"rep": r, "fs": f}

    uv_rows, out_rows, down_rows = uv_ref.shape[1], out_ref.shape[0], down_ref.shape[0]
    half = down_rows // 2

    def slot(kind, q):
        r, f = coords(q)
        if kind == SCALES:
            return scale_all.at[q]
        if kind == MIXER_IN:
            return uv_all.at[f, :, pl.ds(pl.multiple_of(r * uv_rows, uv_rows), uv_rows)]
        if kind == MIXER_OUT:
            return out_all.at[f, tp, pl.ds(pl.multiple_of(r * out_rows, out_rows), out_rows)]
        if kind == GATE:
            return gate_all.at[q]
        if kind == UP:
            return up_all.at[q]
        return down_all.at[q, pl.ds(0 if kind == DOWN_A else half, half)]

    def send(kind, way, hop):
        ref = slot(kind, at_hop(way, hop - 1))
        return pltpu.make_async_remote_copy(
            src_ref=ref, dst_ref=ref, send_sem=ring_send.at[kind, way, hop - 1],
            recv_sem=ring_recv.at[kind, way, hop - 1], device_id=ring_id(way), device_id_type=MESH)

    def wait_hop(kind, way, hop):
        ref = slot(kind, at_hop(way, hop))
        pltpu.make_async_remote_copy(
            src_ref=ref, dst_ref=ref, send_sem=ring_send.at[kind, way, hop - 1],
            recv_sem=ring_recv.at[kind, way, hop - 1], device_id=ring_id(way),
            device_id_type=MESH).wait_recv()

    def on(condition, action):
        if isinstance(condition, bool):
            if condition:
                action()
        else:
            pl.when(condition)(action)

    def begin(kind):
        for way in range(2):
            send(kind, way, 1).start()

    def pump(kind, hop):
        for way in range(2):
            def take(way=way):
                wait_hop(kind, way, hop)
                on(hop < hops[kind][way], lambda: send(kind, way, hop + 1).start())
            on(hop <= hops[kind][way], take)

    def tp_ref(kind, t):
        if kind == TOKENS:
            return tok_all.at[t]
        if kind == OUT_ROWS:
            return out_all.at[:, t]
        return gated_all.at[t]

    def tp_copy(kind, k, t):
        ref = tp_ref(kind, t)
        return pltpu.make_async_remote_copy(
            src_ref=ref, dst_ref=ref, send_sem=tp_send.at[kind, k - 1],
            recv_sem=tp_recv.at[kind, k - 1], device_id={"tp": lax.rem(tp + k, n_tp)},
            device_id_type=MESH)

    def tp_start(kind):
        for k in range(1, n_tp):
            tp_copy(kind, k, tp).start()

    def tp_wait(kind):
        for k in range(1, n_tp):
            tp_copy(kind, k, lax.rem(tp - k + n_tp, n_tp)).wait_recv()

    own = [
        pltpu.make_async_copy(tokens_ref, tok_all.at[tp], local_sem.at[0]),
        pltpu.make_async_copy(scales_ref, slot(SCALES, me), local_sem.at[1]),
        pltpu.make_async_copy(uv_ref, slot(MIXER_IN, me), local_sem.at[2]),
        pltpu.make_async_copy(out_ref, slot(MIXER_OUT, me), local_sem.at[3]),
        pltpu.make_async_copy(gate_ref, gate_all.at[me], local_sem.at[4]),
        pltpu.make_async_copy(up_ref, up_all.at[me], local_sem.at[5]),
        pltpu.make_async_copy(down_ref, down_all.at[me], local_sem.at[6]),
    ]
    for copy in own:
        copy.start()
    barrier = pltpu.get_barrier_semaphore()
    for way in range(2):
        pl.semaphore_signal(barrier, inc=1, device_id=ring_id(way), device_id_type=MESH)
    for k in range(1, n_tp):
        pl.semaphore_signal(barrier, inc=1, device_id={"tp": lax.rem(tp + k, n_tp)},
                            device_id_type=MESH)
    pl.semaphore_wait(barrier, 2 + n_tp - 1)
    for copy in own:
        copy.wait()

    tp_start(TOKENS)
    for kind in (MIXER_IN, MIXER_OUT, SCALES):
        begin(kind)

    def small_step(hop, carry):
        for kind in (MIXER_IN, MIXER_OUT, SCALES):
            pump(kind, hop)
        return carry

    lax.fori_loop(1, far, small_step, 0)
    begin(GATE)
    begin(UP)
    small_step(far, 0)
    tp_start(OUT_ROWS)
    tp_wait(TOKENS)

    span = lower_ref.shape[1]
    groups = lower_ref.shape[0]

    def span_rows(i):
        return pl.ds(pl.multiple_of(i * span, span), span)

    def norm_span(i, gain_ref):
        here = span_rows(i)
        square = jnp.zeros((span, 1), jnp.float32)
        for t in range(n_tp):
            wide = tok_all[t, here, :].astype(jnp.float32)
            square += jnp.sum(wide * wide, axis=-1, keepdims=True)
        inverse = lax.rsqrt(square / (n_tp * own_width) + EPS)
        for f in range(n_fs):
            t, sub = f // per_own, f % per_own
            wide = tok_all[t, here, sub * block:(sub + 1) * block].astype(jnp.float32)
            gain = gain_ref[:, f * block:(f + 1) * block]
            normed[f, here, :] = (wide * inverse * gain).astype(jnp.bfloat16)

    def mixer_span(i, carry):
        here = span_rows(i)
        norm_span(i, pre_gain_ref)
        u_pre = v_pre = None
        for f in range(n_fs):
            source = normed[f, here, :]
            u_term = jnp.dot(source, uv_all[f, 0], preferred_element_type=jnp.float32)
            v_term = jnp.dot(source, uv_all[f, 1], preferred_element_type=jnp.float32)
            u_pre = u_term if f == 0 else u_pre + u_term
            v_pre = v_term if f == 0 else v_pre + v_term
        u_act = jax.nn.gelu(u_pre * u_scale_ref[...])
        v_act = jax.nn.gelu(v_pre * v_scale_ref[...])
        width = v_act.shape[1] // groups
        group_of = lax.broadcasted_iota(jnp.int32, v_act.shape, 1) // width
        centre = jnp.zeros_like(v_act)
        for g in range(groups):
            mean = jnp.sum(jnp.where(group_of == g, v_act, 0.0), axis=-1, keepdims=True) / width
            centre = jnp.where(group_of == g, mean, centre)
        apart = v_act - centre
        square = apart * apart
        inverse = jnp.zeros_like(v_act)
        for g in range(groups):
            spread = jnp.sum(jnp.where(group_of == g, square, 0.0), axis=-1, keepdims=True) / width
            inverse = jnp.where(group_of == g, lax.rsqrt(spread + EPS), inverse)
        v_norm = (apart * inverse * group_gain_ref[...]).astype(jnp.bfloat16)
        mixed = bias_ref[...]
        for g in range(groups):
            term = jnp.dot(lower_ref[g], v_norm, preferred_element_type=jnp.float32)
            mixed = mixed + jnp.where(group_of == g, term, 0.0)
        gated_all[tp, here, :] = (u_act * mixed).astype(jnp.bfloat16)
        return carry

    spans = rows // span
    lax.fori_loop(0, spans, mixer_span, 0)
    tp_start(GATED)
    pump(GATE, 1)
    tp_wait(OUT_ROWS)
    tp_wait(GATED)

    def resid_span(i, carry):
        here = span_rows(i)
        for f in range(n_fs):
            t, sub = f // per_own, f % per_own
            mix = None
            for s in range(n_tp):
                term = jnp.dot(gated_all[s, here, :], out_all[f, s],
                               preferred_element_type=jnp.float32)
                mix = term if s == 0 else mix + term
            mix = (mix * scale_all[f, 0:1, :]).astype(jnp.bfloat16)
            cols = slice(sub * block, (sub + 1) * block)
            tok_all[t, here, cols] = (
                tok_all[t, here, cols].astype(jnp.float32) + mix.astype(jnp.float32)
            ).astype(jnp.bfloat16)
        norm_span(i, ffn_gain_ref)
        return carry

    for k in range(1, n_tp):
        tp_copy(TOKENS, k, tp).wait_send()
    lax.fori_loop(0, spans, resid_span, 0)
    pump(UP, 1)

    chunk = span
    chunks = rows // chunk

    def fold(acc, weights, q):
        r, f = coords(q)

        def body(i, carry):
            here = pl.ds(pl.multiple_of(i * chunk, chunk), chunk)
            term = jnp.dot(normed[f, here, :], weights[q], preferred_element_type=jnp.float32)
            acc[r, here, :] = acc[r, here, :] + term
            return carry

        lax.fori_loop(0, chunks, body, 0)

    gate_acc[...] = jnp.zeros_like(gate_acc)
    up_acc[...] = jnp.zeros_like(up_acc)
    fold(gate_acc, gate_all, me)
    fold(up_acc, up_all, me)

    def fold_hop(acc, weights, kind, hop):
        for way in range(2):
            on(hop <= hops[kind][way],
               lambda way=way: fold(acc, weights, at_hop(way, hop)))

    def ffn_step(hop, carry):
        on(hop > 1, lambda: pump(GATE, hop))
        fold_hop(gate_acc, gate_all, GATE, hop)
        on(hop > 1, lambda: pump(UP, hop))

        def start_down():
            begin(DOWN_A)
            begin(DOWN_B)

        on(hop == far - 1, start_down)
        fold_hop(up_acc, up_all, UP, hop)
        return carry

    lax.fori_loop(1, far + 1, ffn_step, 0)

    def hidden_chunk(i, carry):
        here = pl.ds(pl.multiple_of(i * chunk, chunk), chunk)
        for r in range(n_rep):
            a = gate_acc[r, here, :] * gate_scale_ref[r:r + 1, :]
            b = up_acc[r, here, :] * up_scale_ref[r:r + 1, :]
            hidden[r, here, :] = (a / (1.0 + jnp.exp(-a)) * b).astype(jnp.bfloat16)
        return carry

    lax.fori_loop(0, chunks, hidden_chunk, 0)
    ffn_acc[...] = jnp.zeros_like(ffn_acc)

    def fold_down(q, low, size):
        r, f = coords(q)

        def body(i, carry):
            here = pl.ds(pl.multiple_of(i * chunk, chunk), chunk)
            term = jnp.dot(hidden[r, here, :], down_all[q], preferred_element_type=jnp.float32)
            ffn_acc[f, here, :] = ffn_acc[f, here, :] + term
            return carry

        lax.fori_loop(0, chunks, body, 0)

    def part_copy(f, owner, sender):
        sub = lax.rem(f, per_own)
        return pltpu.make_async_remote_copy(
            src_ref=part.at[f], dst_ref=parts_in.at[sender, sub], send_sem=part_send.at[f],
            recv_sem=part_recv.at[sender, sub], device_id={"tp": owner}, device_id_type=MESH)

    def finish(f):
        def body(i, carry):
            here = pl.ds(pl.multiple_of(i * chunk, chunk), chunk)
            part[f, here, :] = (ffn_acc[f, here, :] * scale_all[f, 1:2, :]).astype(jnp.bfloat16)
            return carry

        lax.fori_loop(0, chunks, body, 0)
        owner = f // per_own
        on(owner != tp, lambda: part_copy(f, owner, tp).start())

    def complete_at(f):
        last = 0
        for r in range(n_rep):
            gap = lax.rem(me - place(r, f) + n_ring, n_ring)
            last = jnp.maximum(last, jnp.minimum(gap, n_ring - gap))
        return last

    fold_down(me, 0, down_rows)

    def down_step(hop, carry):
        pump(DOWN_A, hop)
        pump(DOWN_B, hop)
        fold_down(at_hop(0, hop), 0, down_rows)
        on(hop <= near, lambda: fold_down(at_hop(1, hop), 0, down_rows))

        def finish_if(f, inner):
            on(complete_at(f) == hop, lambda: finish(f))
            return inner

        lax.fori_loop(0, n_fs, finish_if, 0)
        return carry

    lax.fori_loop(1, far + 1, down_step, 0)

    for k in range(1, n_tp):
        sender = lax.rem(tp + k, n_tp)
        for sub in range(per_own):
            part_copy(tp * per_own + sub, tp, sender).wait_recv()

    def close_span(i, carry):
        here = pl.ds(pl.multiple_of(i * chunk, chunk), chunk)
        for sub in range(per_own):
            cols = slice(sub * block, (sub + 1) * block)
            total = part[tp * per_own + sub, here, :].astype(jnp.float32)
            for k in range(1, n_tp):
                total += parts_in[lax.rem(tp + k, n_tp), sub, here, :].astype(jnp.float32)
            total = total.astype(jnp.bfloat16).astype(jnp.float32)
            kept = tok_all[tp, here, cols].astype(jnp.float32)
            result_ref[here, cols] = (kept + total).astype(jnp.bfloat16)
        return carry

    lax.fori_loop(0, chunks, close_span, 0)

    for kind in range(KINDS):
        for way in range(2):
            def sent(hop, carry, kind=kind, way=way):
                send(kind, way, hop).wait_send()
                return carry

            lax.fori_loop(1, hops[kind][way] + 1, sent, 0)
    for kind in (OUT_ROWS, GATED):
        for k in range(1, n_tp):
            tp_copy(kind, k, tp).wait_send()

    def part_sent(f, carry):
        owner = f // per_own
        on(owner != tp, lambda: part_copy(f, owner, tp).wait_send())
        return carry

    lax.fori_loop(0, n_fs, part_sent, 0)


def shards(
    sizes,
    tokens,
    pre_gain,
    u_weight,
    u_scale,
    v_weight,
    v_scale,
    group_gain,
    span_weight,
    span_bias,
    out_weight,
    out_scale,
    ffn_gain,
    gate_weight,
    gate_scale,
    up_weight,
    up_scale,
    down_weight,
    down_scale,
):
    n_rep, n_fs, n_tp = sizes
    n_ring = n_rep * n_fs
    rep = lax.axis_index("rep")

    def share(array, axis):
        width = array.shape[axis] // n_rep
        return lax.dynamic_slice_in_dim(array, rep * width, width, axis).astype(jnp.bfloat16)

    rows, own_width = tokens.shape
    block, local_hidden = gate_weight.shape
    hid = local_hidden // n_rep
    channels = u_weight.shape[1]
    groups, span = span_weight.shape[0], span_weight.shape[1]
    uv = share(jnp.stack([u_weight, v_weight]), 1)
    scales = jnp.stack([out_scale, down_scale])
    bias = jnp.repeat(jnp.transpose(span_bias), channels // groups, axis=1)
    row = lambda vector: vector.reshape(1, -1)
    operands = (
        tokens, scales, uv, share(out_weight, 0), share(gate_weight, 1), share(up_weight, 1),
        share(down_weight, 0), row(pre_gain), row(ffn_gain), row(u_scale), row(v_scale),
        row(group_gain), jnp.tril(span_weight), bias, gate_scale.reshape(n_rep, hid),
        up_scale.reshape(n_rep, hid),
    )
    hbm, vmem = pl.BlockSpec(memory_space=pl.ANY), pl.BlockSpec(memory_space=pltpu.VMEM)
    bf16, f32 = jnp.bfloat16, jnp.float32
    per_own = own_width // block
    steps = n_ring // 2
    return pl.pallas_call(
        functools.partial(layer_kernel, sizes),
        out_shape=jax.ShapeDtypeStruct((rows, own_width), bf16),
        in_specs=[hbm] * 7 + [vmem] * 9,
        out_specs=vmem,
        scratch_shapes=[
            pltpu.VMEM((n_tp, rows, own_width), bf16),
            pltpu.VMEM((n_ring, 2, block), f32),
            pltpu.VMEM((n_fs, 2, block, channels), bf16),
            pltpu.VMEM((n_fs, n_tp, channels, block), bf16),
            pltpu.VMEM((n_ring, block, hid), bf16),
            pltpu.VMEM((n_ring, block, hid), bf16),
            pltpu.VMEM((n_ring, hid, block), bf16),
            pltpu.VMEM((n_fs, rows, block), bf16),
            pltpu.VMEM((n_tp, rows, channels), bf16),
            pltpu.VMEM((n_rep, rows, hid), f32),
            pltpu.VMEM((n_rep, rows, hid), f32),
            pltpu.VMEM((n_rep, rows, hid), bf16),
            pltpu.VMEM((n_fs, rows, block), f32),
            pltpu.VMEM((n_fs, rows, block), bf16),
            pltpu.VMEM((n_tp, per_own, rows, block), bf16),
            pltpu.SemaphoreType.DMA((7,)),
            pltpu.SemaphoreType.DMA((KINDS, 2, steps)),
            pltpu.SemaphoreType.DMA((KINDS, 2, steps)),
            pltpu.SemaphoreType.DMA((3, n_tp - 1)),
            pltpu.SemaphoreType.DMA((3, n_tp - 1)),
            pltpu.SemaphoreType.DMA((n_fs,)),
            pltpu.SemaphoreType.DMA((n_tp, per_own)),
        ],
        compiler_params=pltpu.CompilerParams(
            collective_id=0, has_side_effects=True, vmem_limit_bytes=62 * 1024 * 1024
        ),
    )(*operands)


def solution(mesh):
    placed = (
        P(("rep", "fs"), "tp"),
        P(),
        P("fs", "tp"),
        P("tp"),
        P("fs", "tp"),
        P("tp"),
        P("tp"),
        P("tp", None, None),
        P("tp", None),
        P("tp", "fs"),
        P("fs"),
        P(),
        P("fs", "tp"),
        P("tp"),
        P("fs", "tp"),
        P("tp"),
        P("tp", "fs"),
        P("fs"),
    )
    sizes = (mesh.shape["rep"], mesh.shape["fs"], mesh.shape["tp"])
    return jax.shard_map(
        functools.partial(shards, sizes), mesh=mesh, in_specs=placed, out_specs=P(("rep", "fs"), "tp"), check_vma=False
    )
```

profile of v0, /device:TPU:24, one launch (start us, length us, event | category | flops | bytes accessed | tf_op | source)
XLA Modules:
  0.0 229.5 jit_solution(5766268063579390711)
XLA Ops:
  0.0 0.0 copy-start
  0.0 1.3 pad_maximum_fusion.scales_ref
  1.3 1.4 reshape.30.gate_scale_ref
  2.7 1.4 reshape.31.up_scale_ref
  4.1 1.5 broadcast_select_fusion.lower_ref
  5.6 0.0 copy-done
  5.6 0.6 dynamic-slice_convert_fusion.3.out_ref
  6.2 0.7 broadcast_in_dim.13
  6.9 0.7 copy.20.bias_ref
  7.6 1.6 fusion.1.uv_ref
  9.2 2.3 %dynamic-slice_convert_fusion.2.down_ref = bf16[704,512]{1,0:T(8,128)(2,1)} fusion(f32[1408,512]{1,0:T(8,128)} %param.34, s32[]{:T(128)S(6)} %select_n.17), kind=kLoop, calls=%fused_computation.2 | loop fusion | bytes 1441796 | tf_op jit(solution)/shard_map/convert_element_type | solution.py:438
  11.5 3.7 %dynamic-slice_convert_fusion = (bf16[512,704]{1,0:T(8,128)(2,1)}, bf16[512,704]{1,0:T(8,128)(2,1)}) fusion(f32[512,1408]{1,0:T(8,128)} %param.32, s32[]{:T(128)S(6)} %select_n.17, f32[512,1408]{1,0:T(8,128)} %param.30), kind=kLoop, calls=%fused_computation | loop fusion | bytes 2883588 | tf_op jit(solution)/shard_map/convert_element_type | solution.py:438
  15.3 212.4 %shard_map.172 = bf16[512,512]{1,0:T(8,128)(2,1)} custom-call(bf16[512,512]{1,0:T(8,128)(2,1)} %tokens_ref.1, f32[2,512]{1,0:T(2,128)} %pad_maximum_fusion.scales_ref, bf16[2,256,128]{2,1,0:T(8,128)(2,1)} %fusion.1.uv_ref, bf16[64,512]{1,0:T(8,128)(2,1)} %dynamic-slice_convert_fusion.3.out_ref, bf16[512,704]{1,0:T(8,128)(2,1)} %get-tuple-element.6.gate_ref, ...), custom_call_target="tpu_custom_call" | custom-call | tf_op jit(solution)/shard_map/pallas_call | solution.py:459
  227.7 1.9 copy.22
  (1 shorter events, 0.0 us)
Async XLA Ops:
  0.0 5.6 %copy-start = (f32[128,512]{1,0:T(8,128)S(1)}, f32[128,512]{1,0:T(8,128)}, u32[]{:S(2)}) copy-start(f32[128,512]{1,0:T(8,128)} %param.27) | copy-start | bytes 786436
where the time goes:
time: 230 us
  Pallas kernels  212 us (92%)
  local copies, waits for them, and re-layouts  12.7 us (6%)
  other arithmetic  4.46 us (2%)
    pallas_call x1, Pallas kernels, shards(): pl.pallas_call(functools.partial(layer_kernel, sizes), out_shape=jax.Shap...  212 us
    convert_element_type x3, local copies, waits for them, and re-layouts, share(): lax.dynamic_slice_in_dim(array, rep * width, width, axis)  6.65 us

commit v1 on v0

v1 whole, which is shorter than its diff:
```python
import functools

import jax
import jax.numpy as jnp
from jax import lax
from jax.experimental import pallas as pl
from jax.experimental.pallas import tpu as pltpu
from jax.sharding import PartitionSpec as P

EPS = 0.02
MESH = pl.DeviceIdType.MESH
LANES = 128
UV, GU0, GU1, DN0, DN1 = range(5)
KINDS = 5
TOK, GATED, OWN, PAIR = range(4)
CHUNK = 256


def on(condition, action):
    if isinstance(condition, bool):
        if condition:
            action()
    else:
        pl.when(condition)(action)


def flip(a, d, size):
    total, bit = 0, 1
    while bit < size:
        total = total + lax.rem(lax.div(a, jnp.int32(bit)) + lax.div(jnp.int32(d), jnp.int32(bit)), jnp.int32(2)) * bit
        bit *= 2
    return total


def loop(low, high, body):
    def step(i, carry):
        body(i)
        return carry

    lax.fori_loop(low, high, step, 0)


def layer_kernel(
    sizes,
    tokens_ref,
    u_ref,
    v_ref,
    out_ref,
    gate_ref,
    up_ref,
    down_ref,
    out_scale_ref,
    down_scale_ref,
    pre_gain_ref,
    ffn_gain_ref,
    u_scale_ref,
    v_scale_ref,
    group_gain_ref,
    span_ref,
    bias_ref,
    gate_scale_ref,
    up_scale_ref,
    result_ref,
    u_f,
    v_f,
    out_f,
    gate_f,
    up_f,
    down_f,
    out_own,
    gu_own,
    down_own,
    tok_all,
    uv_all,
    out_all,
    scale_all,
    gated_all,
    resid_all,
    normed,
    gu_all,
    down_all,
    gu_acc,
    hidden,
    part,
    mate_in,
    x_in,
    pair_in,
    local_sem,
    z_send,
    z_recv,
    y_send,
    y_recv,
    e_send,
    e_recv,
    p_send,
    p_recv,
    o_send,
    o_recv,
    s_send,
    s_recv,
    m_send,
    m_recv,
    x_send,
    x_recv,
    q_send,
    q_recv,
):
    n_rep, n_fs, n_tp = sizes
    n_x = n_tp // 2
    rows, own_width = tokens_ref.shape
    block = gate_ref.shape[0]
    per_own = own_width // block
    hid = gate_ref.shape[1] // 2
    main = hid // LANES * LANES
    channels = u_ref.shape[1]
    groups, span = span_ref.shape[0], span_ref.shape[1]
    spans = rows // span
    total_rows = 2 * rows
    chunks = total_rows // CHUNK
    half_chunks = chunks // 2
    rep, fs, tp = lax.axis_index("rep"), lax.axis_index("fs"), lax.axis_index("tp")
    two = jnp.int32(2)
    member = lax.rem(fs, two)
    core, xi = lax.rem(tp, two), lax.div(tp, two)
    mate = tp + 1 - 2 * core
    pair = fs + 1 - 2 * member
    owner = lax.div(fs, jnp.int32(per_own))
    owner_sub = lax.rem(fs, jnp.int32(per_own))

    def copy(src, dst, send_sem, recv_sem, **device):
        return pltpu.make_async_remote_copy(
            src_ref=src, dst_ref=dst, send_sem=send_sem, recv_sem=recv_sem, device_id=device, device_id_type=MESH)

    def rows_at(i, size):
        return pl.ds(pl.multiple_of(i * size, size), size)

    k_uv, k_gu, k_dn = block // n_rep, block // n_rep // 2, hid // n_rep // 2

    def w_rows(kind, r):
        if kind == UV:
            return pl.ds(pl.multiple_of(r * k_uv, k_uv), k_uv)
        if kind in (GU0, GU1):
            return pl.ds(pl.multiple_of((2 * r + (kind - GU0)) * k_gu, k_gu), k_gu)
        return pl.ds(pl.multiple_of((2 * r + (kind - DN0)) * k_dn, k_dn), k_dn)

    def w_slot(kind, f, r):
        ref = uv_all if kind == UV else gu_all if kind in (GU0, GU1) else down_all
        return ref.at[f, w_rows(kind, r)]

    def w_source(kind, g):
        if kind == UV:
            return w_slot(UV, fs, rep)
        ref = gu_own if kind in (GU0, GU1) else down_own
        return ref.at[lax.rem(g, two), w_rows(kind, rep)]

    def z_copy(kind, d):
        g = flip(fs, d, n_fs)
        return copy(w_source(kind, g), w_slot(kind, fs, rep), z_send.at[kind, d - 1], z_recv.at[kind, d - 1], fs=g)

    def y_copy(kind, d, e):
        slot = w_slot(kind, flip(fs, d, n_fs), rep)
        return copy(slot, slot, y_send.at[kind, d - 1, e - 1], y_recv.at[kind, d - 1, e - 1],
                    rep=lax.rem(rep + e, jnp.int32(n_rep)))

    def z_start(kind):
        loop(1, n_fs, lambda d: z_copy(kind, d).start())

    def y_relay(kind, d):
        slot = w_slot(kind, flip(fs, d, n_fs), rep)
        copy(slot, slot, z_send.at[kind, d - 1], z_recv.at[kind, d - 1], fs=pair).wait_recv()
        for e in range(1, n_rep):
            y_copy(kind, d, e).start()

    def y_ready(kind, d):
        for e in range(1, n_rep):
            slot = w_slot(kind, flip(fs, d, n_fs), lax.rem(rep - e + n_rep, jnp.int32(n_rep)))
            copy(slot, slot, y_send.at[kind, d - 1, e - 1], y_recv.at[kind, d - 1, e - 1],
                 rep=lax.rem(rep + 1, jnp.int32(n_rep))).wait_recv()

    def e_slot(kind, i, t):
        here = rows_at(i, span)
        if kind == TOK:
            return tok_all.at[t, here]
        if kind == GATED:
            return gated_all.at[t, here]
        return resid_all.at[member if kind == OWN else 1 - member, t, here]

    def x_peer(dx):
        return 2 * flip(xi, dx, n_x) + core

    def e_copy(kind, i, t, k, to):
        slot = e_slot(kind, i, t)
        return copy(slot, slot, e_send.at[kind, i, k], e_recv.at[kind, i, t], tp=to)

    def e_list(kind, i):
        out = [e_copy(kind, i, tp, 0, mate)]
        for dx in range(1, n_x):
            out.append(e_copy(kind, i, tp, dx, x_peer(dx)))
        return out

    def e_push(kind, i):
        for c in e_list(kind, i):
            c.start()

    def e_wait(kind, i, t):
        e_copy(kind, i, t, 0, mate).wait_recv()

    def e_relay(kind, i):
        for dx in range(1, n_x):
            e_wait(kind, i, x_peer(dx))
            e_copy(kind, i, x_peer(dx), n_x - 1 + dx, mate).start()

    def e_finish(kind, i):
        for dx in range(n_x):
            e_wait(kind, i, 2 * flip(xi, dx, n_x) + 1 - core)

    def e_sent(kind, i):
        for c in e_list(kind, i):
            c.wait_send()
        for dx in range(1, n_x):
            e_copy(kind, i, x_peer(dx), n_x - 1 + dx, mate).wait_send()

    def p_copy(i, which):
        slot = resid_all.at[which, tp, rows_at(i, span)]
        return copy(slot, slot, p_send.at[i], p_recv.at[i], fs=pair)

    def o_copy(d):
        g = flip(fs, d, n_fs)
        return copy(out_own, out_all.at[tp, owner_sub], o_send.at[d], o_recv.at[tp, owner_sub], fs=g, tp=owner)

    def o_each(action):
        def body(d):
            on(jnp.logical_or(d > 0, owner != tp), lambda: action(d))

        loop(0, n_fs, body)

    def s_copy(d, which):
        g = flip(fs, d, n_fs)
        src = (out_scale_ref, down_scale_ref)[which]
        return copy(src, scale_all.at[which, owner_sub], s_send.at[which, d - 1], s_recv.at[which, owner_sub], fs=g)

    loads = [
        pltpu.make_async_copy(src, dst, local_sem.at[i])
        for i, (src, dst) in enumerate((
            (tokens_ref, tok_all.at[tp]), (u_ref, u_f), (v_ref, v_f), (out_ref, out_f), (gate_ref, gate_f),
            (up_ref, up_f), (down_ref, down_f)))
    ]
    for load in loads:
        load.start()

    barrier = pltpu.get_barrier_semaphore()

    def greet(**device):
        pl.semaphore_signal(barrier, inc=1, device_id=device, device_id_type=MESH)

    greet(tp=mate)
    for dx in range(1, n_x):
        greet(tp=x_peer(dx))
    loop(1, n_fs, lambda d: greet(fs=flip(fs, d, n_fs)))
    for e in range(1, n_rep):
        greet(rep=lax.rem(rep + e, jnp.int32(n_rep)))

    def greet_source(i):
        f, t = tp * per_own + lax.div(i, jnp.int32(n_tp)), lax.rem(i, jnp.int32(n_tp))
        on(jnp.logical_or(f != fs, t != tp), lambda: greet(fs=f, tp=t))

    loop(0, per_own * n_tp, greet_source)
    pl.semaphore_wait(barrier, 1 + (n_x - 1) + (n_fs - 1) + (n_rep - 1) + jnp.where(owner == tp, n_fs - 1, n_fs))

    loads[0].wait()
    loop(0, spans, lambda i: e_push(TOK, i))
    loads[1].wait()
    loads[2].wait()
    uv_all[fs, :, 0:channels] = u_f[...].astype(jnp.bfloat16)
    uv_all[fs, :, channels:2 * channels] = v_f[...].astype(jnp.bfloat16)
    z_start(UV)
    loads[3].wait()
    out_own[...] = out_f[...].astype(jnp.bfloat16)

    def keep_own():
        out_all[tp, owner_sub] = out_f[...].astype(jnp.bfloat16)
        scale_all[0, owner_sub] = out_scale_ref[...]
        scale_all[1, owner_sub] = down_scale_ref[...]

    on(owner == tp, keep_own)
    o_each(lambda d: o_copy(d).start())

    def s_each(action):
        def body(d):
            for which in range(2):
                action(s_copy(d, which))

        on(owner == tp, lambda: loop(1, n_fs, body))

    s_each(lambda c: c.start())

    low = lax.broadcasted_iota(jnp.int32, (1, LANES), 1) < LANES // 2
    unit = 64

    def swap(value):
        return pltpu.roll(value, LANES // 2, 1)

    loads[4].wait()
    loads[5].wait()

    def cast_gu(i):
        here = rows_at(i, unit)
        for member_of in range(2):
            first = member_of * (main + LANES)
            gu_own[member_of, here, 0:main] = gate_f[here, first:first + main].astype(jnp.bfloat16)
            gu_own[member_of, here, main:2 * main] = up_f[here, first:first + main].astype(jnp.bfloat16)
        g, u = gate_f[here, main:main + LANES], up_f[here, main:main + LANES]
        gu_own[0, here, 2 * main:] = jnp.where(low, g, swap(u)).astype(jnp.bfloat16)
        gu_own[1, here, 2 * main:] = jnp.where(low, swap(g), u).astype(jnp.bfloat16)

    loop(0, block // unit, cast_gu)
    z_start(GU0)
    keep_gu = pltpu.make_async_copy(gu_own.at[member], gu_all.at[fs], local_sem.at[7])
    keep_gu.start()
    loads[6].wait()

    def cast_down(i):
        here = rows_at(i, unit)
        down_own[0, here] = down_f[here].astype(jnp.bfloat16)
        there = jnp.where(i < main // unit, i + (main + LANES) // unit, main // unit + 1)
        down_own[1, here] = down_f[rows_at(there, unit)].astype(jnp.bfloat16)

    loop(0, hid // unit, cast_down)
    keep_down = pltpu.make_async_copy(down_own.at[member], down_all.at[fs], local_sem.at[8])
    keep_down.start()

    loop(0, spans, lambda i: e_relay(TOK, i))
    loop(1, n_fs, lambda d: y_relay(UV, d))
    loop(1, n_fs, lambda d: y_ready(UV, d))

    eye = lax.broadcasted_iota(jnp.int32, (span, span), 0) == lax.broadcasted_iota(jnp.int32, (span, span), 1)
    tril = lax.broadcasted_iota(jnp.int32, (span, span), 0) >= lax.broadcasted_iota(jnp.int32, (span, span), 1)

    def mixer_span(i):
        e_finish(TOK, i)
        here = rows_at(i, span)
        square = jnp.zeros((span, 1), jnp.float32)
        for t in range(n_tp):
            wide = tok_all[t, here, :].astype(jnp.float32)
            square += jnp.sum(wide * wide, axis=-1, keepdims=True)
        inverse = lax.rsqrt(square / (n_tp * own_width) + EPS)
        pre = None
        for f in range(n_fs):
            t, sub = f // per_own, f % per_own
            wide = tok_all[t, here, sub * block:(sub + 1) * block].astype(jnp.float32)
            source = (wide * inverse * pre_gain_ref[:, f * block:(f + 1) * block]).astype(jnp.bfloat16)
            term = jnp.dot(source, uv_all[f], preferred_element_type=jnp.float32)
            pre = term if f == 0 else pre + term
        u_act = jax.nn.gelu(pre[:, :channels] * u_scale_ref[...])
        v_act = jax.nn.gelu(pre[:, channels:] * v_scale_ref[...])
        width = channels // groups
        group_of = lax.broadcasted_iota(jnp.int32, v_act.shape, 1) // width
        centre = jnp.zeros_like(v_act)
        for g in range(groups):
            mean = jnp.sum(jnp.where(group_of == g, v_act, 0.0), axis=-1, keepdims=True) / width
            centre = jnp.where(group_of == g, mean, centre)
        apart = v_act - centre
        square = apart * apart
        inverse = jnp.zeros_like(v_act)
        for g in range(groups):
            spread = jnp.sum(jnp.where(group_of == g, square, 0.0), axis=-1, keepdims=True) / width
            inverse = jnp.where(group_of == g, lax.rsqrt(spread + EPS), inverse)
        v_norm = (apart * inverse * group_gain_ref[...]).astype(jnp.bfloat16)
        mixed = jnp.zeros_like(v_act)
        for g in range(groups):
            lower = jnp.where(tril, span_ref[g].astype(jnp.float32), 0.0).astype(jnp.bfloat16)
            bias = jnp.sum(jnp.where(eye, bias_ref[g:g + 1, :], 0.0), axis=1, keepdims=True)
            term = jnp.dot(lower, v_norm, preferred_element_type=jnp.float32) + bias
            mixed = jnp.where(group_of == g, term, mixed)
        gated_all[tp, here, :] = (u_act * mixed).astype(jnp.bfloat16)
        e_push(GATED, i)

    loop(0, spans, mixer_span)
    loop(0, spans, lambda i: e_relay(GATED, i))

    def out_arrived(i):
        sub, t = lax.div(i, jnp.int32(n_tp)), lax.rem(i, jnp.int32(n_tp))
        on(jnp.logical_or(tp * per_own + sub != fs, t != tp),
           lambda: copy(out_own, out_all.at[t, sub], o_send.at[0], o_recv.at[t, sub], fs=pair, tp=mate).wait_recv())

    loop(0, per_own * n_tp, out_arrived)

    def scale_arrived(sub):
        def take():
            for which in range(2):
                copy(out_scale_ref, scale_all.at[which, sub], s_send.at[which, 0], s_recv.at[which, sub],
                     fs=pair).wait_recv()

        on(tp * per_own + sub != fs, take)

    loop(0, per_own, scale_arrived)

    def resid_span(i):
        e_finish(GATED, i)
        here = rows_at(i, span)
        for sub in range(per_own):
            mix = None
            for s in range(n_tp):
                term = jnp.dot(gated_all[s, here, :], out_all[s, sub], preferred_element_type=jnp.float32)
                mix = term if s == 0 else mix + term
            mix = (mix * scale_all[0, sub]).astype(jnp.bfloat16)
            cols = slice(sub * block, (sub + 1) * block)
            resid_all[member, tp, here, cols] = (
                tok_all[tp, here, cols].astype(jnp.float32) + mix.astype(jnp.float32)).astype(jnp.bfloat16)
        e_push(OWN, i)
        p_copy(i, member).start()

    loop(0, spans, resid_span)
    for kind in (GU1, DN0, DN1):
        z_start(kind)

    def norm_span(which, i):
        here = rows_at(i, span)
        square = jnp.zeros((span, 1), jnp.float32)
        for t in range(n_tp):
            wide = resid_all[which, t, here, :].astype(jnp.float32)
            square += jnp.sum(wide * wide, axis=-1, keepdims=True)
        inverse = lax.rsqrt(square / (n_tp * own_width) + EPS)
        there = rows_at(which * spans + i, span)
        for f in range(n_fs):
            t, sub = f // per_own, f % per_own
            wide = resid_all[which, t, here, sub * block:(sub + 1) * block].astype(jnp.float32)
            gain = ffn_gain_ref[:, f * block:(f + 1) * block]
            normed[f, there, :] = (wide * inverse * gain).astype(jnp.bfloat16)

    loop(0, spans, lambda i: e_relay(OWN, i))

    def own_span(i):
        e_finish(OWN, i)
        norm_span(member, i)

    loop(0, spans, own_span)
    loop(1, n_fs, lambda d: y_relay(GU0, d))

    def pair_span(i):
        p_copy(i, 1 - member).wait_recv()
        e_push(PAIR, i)

    loop(0, spans, pair_span)
    loop(0, spans, lambda i: e_relay(PAIR, i))

    def other_span(i):
        e_finish(PAIR, i)
        norm_span(1 - member, i)

    loop(0, spans, other_span)

    keep_gu.wait()

    def first_gu(i):
        here = rows_at(i, CHUNK)
        gu_acc[here, :] = jnp.dot(normed[fs, here, :], gu_all[fs], preferred_element_type=jnp.float32)

    loop(0, chunks, first_gu)
    loop(1, n_fs, lambda d: y_relay(GU1, d))

    def fold_gu(d):
        y_ready(GU0, d)
        y_ready(GU1, d)
        f = flip(fs, d, n_fs)

        def body(i):
            here = rows_at(i, CHUNK)
            gu_acc[here, :] += jnp.dot(normed[f, here, :], gu_all[f], preferred_element_type=jnp.float32)

        loop(0, chunks, body)

    loop(1, n_fs, fold_gu)

    second = member == 1

    def main_scale(ref):
        return jnp.where(second, ref[:, main + LANES:], ref[:, 0:main])

    gate_main, up_main = main_scale(gate_scale_ref), main_scale(up_scale_ref)
    gs, us = gate_scale_ref[:, main:main + LANES], up_scale_ref[:, main:main + LANES]
    last_scale = jnp.where(second, jnp.where(low, swap(gs), us), jnp.where(low, gs, swap(us)))

    def hidden_chunk(i):
        here = rows_at(i, 64)
        a = gu_acc[here, 0:main] * gate_main
        b = gu_acc[here, main:2 * main] * up_main
        hidden[here, 0:main] = (a / (1.0 + jnp.exp(-a)) * b).astype(jnp.bfloat16)
        a = gu_acc[here, 2 * main:] * last_scale
        b = swap(a)
        last = (a / (1.0 + jnp.exp(-a)) * b).astype(jnp.bfloat16)
        hidden[here, main:hid] = last[:, 0:hid - main]

    loop(0, total_rows // 64, hidden_chunk)
    keep_down.wait()

    def block_at(k):
        return fs - member + 0 if k is None else flip(fs - member, k, n_fs)

    def places(k):
        b = block_at(k)
        own = lax.div(b, jnp.int32(per_own))
        return b, lax.rem(own, two), lax.div(own, two), lax.rem(b, jnp.int32(per_own)), own

    def m_copy(k, j):
        b, oc, ox, sub, own = places(k)
        here = rows_at(j, CHUNK)
        return copy(part.at[b, here], mate_in.at[ox, sub, here], m_send.at[b, j], m_recv.at[ox, sub, j], tp=mate)

    def x_copy(k, j):
        b, oc, ox, sub, own = places(k)
        here = rows_at(j, CHUNK)
        d = flip(xi, ox, n_x)
        return copy(part.at[b, here], x_in.at[d - 1, sub, here], x_send.at[b, j], x_recv.at[d - 1, sub, j], tp=own)

    def q_copy(k, j):
        b, oc, ox, sub, own = places(k)
        src = part.at[b, rows_at((1 - member) * half_chunks + j, CHUNK)]
        return copy(src, pair_in.at[sub, rows_at(j, CHUNK)], q_send.at[sub, j], q_recv.at[sub, j], fs=pair)

    def down_one(k):
        b, oc, ox, sub, own = places(k)
        d = flip(member, k, n_fs)

        def ready():
            y_ready(DN0, d)
            y_ready(DN1, d)

        on(d > 0, ready)

        def body(j):
            here = rows_at(j, CHUNK)
            part[b, here, :] = jnp.dot(hidden[here, :], down_all[b], preferred_element_type=jnp.float32).astype(
                jnp.bfloat16)
            on(core != oc, lambda: m_copy(k, j).start())

        loop(0, chunks, body)

    def across(k):
        b, oc, ox, sub, own = places(k)

        def body(j):
            here = rows_at(j, CHUNK)
            m_copy(k, j).wait_recv()
            part[b, here, :] = (part[b, here, :].astype(jnp.float32)
                                + mate_in[ox, sub, here, :].astype(jnp.float32)).astype(jnp.bfloat16)
            on(xi != ox, lambda: x_copy(k, j).start())

        on(core == oc, lambda: loop(0, chunks, body))

    def collect(k):
        b, oc, ox, sub, own = places(k)

        def body(jj):
            j = lax.rem((1 - member) * half_chunks + jj, jnp.int32(chunks))
            here = rows_at(j, CHUNK)
            total = part[b, here, :].astype(jnp.float32)
            for dx in range(1, n_x):
                copy(part.at[b, here], x_in.at[dx - 1, sub, here], x_send.at[b, j], x_recv.at[dx - 1, sub, j],
                     tp=mate).wait_recv()
                total += x_in[dx - 1, sub, here, :].astype(jnp.float32)
            part[b, here, :] = total.astype(jnp.bfloat16)
            on(jj < half_chunks, lambda: q_copy(k, jj).start())

        on(own == tp, lambda: loop(0, chunks, body))

    def relay_down(k):
        d = flip(member, k, n_fs)

        def go():
            y_relay(DN0, d)
            y_relay(DN1, d)

        on(d > 0, go)

    def down_step(step):
        on(step < n_fs, lambda: relay_down(step))
        on(jnp.logical_and(step >= 1, step < n_fs + 1), lambda: down_one(step - 1))
        on(jnp.logical_and(step >= 2, step < n_fs + 2), lambda: across(step - 2))
        on(step >= 3, lambda: collect(step - 3))

    loop(0, n_fs + 3, down_step)

    for sub in range(per_own):
        b = tp * per_own + sub
        cols = slice(sub * block, (sub + 1) * block)

        def close(j, b=b, sub=sub, cols=cols):
            here = rows_at(j, CHUNK)
            copy(part.at[b, here], pair_in.at[sub, here], q_send.at[sub, j], q_recv.at[sub, j], fs=pair).wait_recv()
            mine = rows_at(member * half_chunks + j, CHUNK)
            total = part[b, mine, :].astype(jnp.float32) + pair_in[sub, here, :].astype(jnp.float32)
            total = (total * scale_all[1, sub]).astype(jnp.bfloat16).astype(jnp.float32)
            kept = resid_all[member, tp, here, cols].astype(jnp.float32)
            result_ref[here, cols] = (kept + total).astype(jnp.bfloat16)

        loop(0, half_chunks, close)

    for kind in range(KINDS):
        def sent(d, kind=kind):
            z_copy(kind, d).wait_send()
            for e in range(1, n_rep):
                y_copy(kind, d, e).wait_send()

        loop(1, n_fs, sent)

    def spans_sent(i):
        for kind in range(4):
            e_sent(kind, i)
        p_copy(i, member).wait_send()

    loop(0, spans, spans_sent)
    o_each(lambda d: o_copy(d).wait_send())
    s_each(lambda c: c.wait_send())

    def parts_sent(k):
        b, oc, ox, sub, own = places(k)

        def body(j):
            on(core != oc, lambda: m_copy(k, j).wait_send())
            on(jnp.logical_and(core == oc, xi != ox), lambda: x_copy(k, j).wait_send())
            on(jnp.logical_and(own == tp, j < half_chunks), lambda: q_copy(k, j).wait_send())

        loop(0, chunks, body)

    loop(0, n_fs, parts_sent)


def shards(
    sizes,
    tokens,
    pre_gain,
    u_weight,
    u_scale,
    v_weight,
    v_scale,
    group_gain,
    span_weight,
    span_bias,
    out_weight,
    out_scale,
    ffn_gain,
    gate_weight,
    gate_scale,
    up_weight,
    up_scale,
    down_weight,
    down_scale,
):
    n_rep, n_fs, n_tp = sizes
    n_x = n_tp // 2
    extra = (LANES - gate_weight.shape[1]) % (2 * LANES)
    if extra:
        gate_weight, up_weight = (jnp.pad(w, ((0, 0), (0, extra))) for w in (gate_weight, up_weight))
        gate_scale, up_scale = (jnp.pad(s, (0, extra)) for s in (gate_scale, up_scale))
        down_weight = jnp.pad(down_weight, ((0, extra), (0, 0)))
    rows, own_width = tokens.shape
    block, local_hidden = gate_weight.shape
    hid = local_hidden // 2
    channels = u_weight.shape[1]
    per_own = own_width // block
    spans = rows // span_weight.shape[1]
    chunks = 2 * rows // CHUNK
    row = lambda vector: vector.reshape(1, -1)
    operands = (
        tokens, u_weight, v_weight, out_weight, gate_weight, up_weight, down_weight, row(out_scale), row(down_scale),
        row(pre_gain), row(ffn_gain), row(u_scale), row(v_scale), row(group_gain), span_weight, span_bias,
        row(gate_scale), row(up_scale),
    )
    hbm, vmem = pl.BlockSpec(memory_space=pl.ANY), pl.BlockSpec(memory_space=pltpu.VMEM)
    bf16, f32 = jnp.bfloat16, jnp.float32
    dma = lambda *shape: pltpu.SemaphoreType.DMA(shape)
    return pl.pallas_call(
        functools.partial(layer_kernel, sizes),
        out_shape=jax.ShapeDtypeStruct((rows, own_width), bf16),
        in_specs=[hbm] * 7 + [vmem] * 11,
        out_specs=vmem,
        scratch_shapes=[
            pltpu.VMEM((block, channels), f32),
            pltpu.VMEM((block, channels), f32),
            pltpu.VMEM((channels, block), f32),
            pltpu.VMEM((block, local_hidden), f32),
            pltpu.VMEM((block, local_hidden), f32),
            pltpu.VMEM((local_hidden, block), f32),
            pltpu.VMEM((channels, block), bf16),
            pltpu.VMEM((2, block, 2 * hid), bf16),
            pltpu.VMEM((2, hid, block), bf16),
            pltpu.VMEM((n_tp, rows, own_width), bf16),
            pltpu.VMEM((n_fs, block, 2 * channels), bf16),
            pltpu.VMEM((n_tp, per_own, channels, block), bf16),
            pltpu.VMEM((2, per_own, 1, block), f32),
            pltpu.VMEM((n_tp, rows, channels), bf16),
            pltpu.VMEM((2, n_tp, rows, own_width), bf16),
            pltpu.VMEM((n_fs, 2 * rows, block), bf16),
            pltpu.VMEM((n_fs, block, 2 * hid), bf16),
            pltpu.VMEM((n_fs, hid, block), bf16),
            pltpu.VMEM((2 * rows, 2 * hid), f32),
            pltpu.VMEM((2 * rows, hid), bf16),
            pltpu.VMEM((n_fs, 2 * rows, block), bf16),
            pltpu.VMEM((n_x, per_own, 2 * rows, block), bf16),
            pltpu.VMEM((n_x - 1, per_own, 2 * rows, block), bf16),
            pltpu.VMEM((per_own, rows, block), bf16),
            dma(9),
            dma(KINDS, n_fs - 1),
            dma(KINDS, n_fs - 1),
            dma(KINDS, n_fs - 1, n_rep - 1),
            dma(KINDS, n_fs - 1, n_rep - 1),
            dma(4, spans, n_tp - 1),
            dma(4, spans, n_tp),
            dma(spans),
            dma(spans),
            dma(n_fs),
            dma(n_tp, per_own),
            dma(2, n_fs - 1),
            dma(2, per_own),
            dma(n_fs, chunks),
            dma(n_x, per_own, chunks),
            dma(n_fs, chunks),
            dma(n_x - 1, per_own, chunks),
            dma(per_own, chunks // 2),
            dma(per_own, chunks // 2),
        ],
        compiler_params=pltpu.CompilerParams(
            collective_id=0, has_side_effects=True, vmem_limit_bytes=63 * 1024 * 1024
        ),
    )(*operands)


def solution(mesh):
    placed = (
        P(("rep", "fs"), "tp"),
        P(),
        P("fs", "tp"),
        P("tp"),
        P("fs", "tp"),
        P("tp"),
        P("tp"),
        P("tp", None, None),
        P("tp", None),
        P("tp", "fs"),
        P("fs"),
        P(),
        P("fs", "tp"),
        P("tp"),
        P("fs", "tp"),
        P("tp"),
        P("tp", "fs"),
        P("fs"),
    )
    sizes = (mesh.shape["rep"], mesh.shape["fs"], mesh.shape["tp"])
    return jax.shard_map(
        functools.partial(shards, sizes), mesh=mesh, in_specs=placed, out_specs=P(("rep", "fs"), "tp"), check_vma=False
    )
```

time: 230 us -> 195 us (0.85)
  Pallas kernels: 212 us -> 191 us
  local copies, waits for them, and re-layouts: 12.7 us -> 4.45 us
  other arithmetic: 4.46 us -> 0 us
    pallas_call x1, Pallas kernels: 212 us -> 191 us  [shards(): pl.pallas_call(functools.partial(layer_kernel, sizes), out_shape=jax.Shap...]
    convert_element_type x3 -> x0, local copies, waits for them, and re-layouts: 6.65 us -> none  [share(): lax.dynamic_slice_in_dim(array, rep * width, width, axis)]
where the time goes in v1:
time: 195 us
  Pallas kernels  191 us (98%)
  local copies, waits for them, and re-layouts  4.45 us (2%)
    pallas_call x1, Pallas kernels, shards(): pl.pallas_call(functools.partial(layer_kernel, sizes), out_shape=jax.Shap...  191 us

profile of v1, /device:TPU:24, one launch (start us, length us, event | category | flops | bytes accessed | tf_op | source)
XLA Modules:
  0.0 195.2 jit_solution(6991775682919538941)
XLA Ops:
  0.0 1.3 reshape.34.gate_scale_ref
  1.3 1.3 reshape.35.up_scale_ref
  2.6 190.7 %shard_map.172 = bf16[512,512]{1,0:T(8,128)(2,1)} custom-call(bf16[512,512]{1,0:T(8,128)(2,1)} %tokens_ref.1, f32[512,128]{1,0:T(8,128)} %u_ref.1, f32[512,128]{1,0:T(8,128)} %v_ref.1, f32[128,512]{1,0:T(8,128)} %out_ref.1, f32[512,1408]{1,0:T(8,128)} %gate_ref.1, f32[512,1408]{1,0:T(8,128)} %up_ref.1, f32[1408,512]{1,0:T(8,128)} %down_ref.1, ...), custom_call_target="tpu_custom_call" | custom-call | tf_op jit(solution)/shard_map/pallas_call | solution.py:673
  193.3 1.9 copy.20

commit v2 on v1

--- a/solution.py
+++ b/solution.py
@@ -10,8 +10,7 @@
 EPS = 0.02
 MESH = pl.DeviceIdType.MESH
 LANES = 128
-UV, GU0, GU1, DN0, DN1 = range(5)
-KINDS = 5
+UV, OUT, GU0, GU1, DN = range(5)
 TOK, GATED, OWN, PAIR = range(4)
 CHUNK = 256
 
@@ -67,11 +66,11 @@
     gate_f,
     up_f,
     down_f,
-    out_own,
     gu_own,
     down_own,
     tok_all,
     uv_all,
+    out_gather,
     out_all,
     scale_all,
     gated_all,
@@ -111,6 +110,9 @@
     block = gate_ref.shape[0]
     per_own = own_width // block
     hid = gate_ref.shape[1] // 2
+    pieces, width_down = down_own.shape[1], down_own.shape[3]
+    per_owner = per_own * pieces
+    units = n_fs * pieces
     main = hid // LANES * LANES
     channels = u_ref.shape[1]
     groups, span = span_ref.shape[0], span_ref.shape[1]
@@ -134,47 +136,53 @@
     def rows_at(i, size):
         return pl.ds(pl.multiple_of(i * size, size), size)
 
-    k_uv, k_gu, k_dn = block // n_rep, block // n_rep // 2, hid // n_rep // 2
-
     def w_rows(kind, r):
-        if kind == UV:
-            return pl.ds(pl.multiple_of(r * k_uv, k_uv), k_uv)
         if kind in (GU0, GU1):
-            return pl.ds(pl.multiple_of((2 * r + (kind - GU0)) * k_gu, k_gu), k_gu)
-        return pl.ds(pl.multiple_of((2 * r + (kind - DN0)) * k_dn, k_dn), k_dn)
-
-    def w_slot(kind, f, r):
-        ref = uv_all if kind == UV else gu_all if kind in (GU0, GU1) else down_all
+            size = block // n_rep // 2
+            return pl.ds(pl.multiple_of((2 * r + (kind - GU0)) * size, size), size)
+        size = (block if kind == UV else channels if kind == OUT else hid) // n_rep
+        return pl.ds(pl.multiple_of(r * size, size), size)
+
+    def w_slot(kind, f, r, p=0):
+        if kind == DN:
+            return down_all.at[f * pieces + p, w_rows(kind, r)]
+        ref = uv_all if kind == UV else out_gather if kind == OUT else gu_all
         return ref.at[f, w_rows(kind, r)]
 
-    def w_source(kind, g):
-        if kind == UV:
-            return w_slot(UV, fs, rep)
-        ref = gu_own if kind in (GU0, GU1) else down_own
-        return ref.at[lax.rem(g, two), w_rows(kind, rep)]
-
-    def z_copy(kind, d):
+    def w_source(kind, g, p=0):
+        if kind in (UV, OUT):
+            return w_slot(kind, fs, rep)
+        if kind == DN:
+            return down_own.at[lax.rem(g, two), p, w_rows(kind, rep)]
+        return gu_own.at[lax.rem(g, two), w_rows(kind, rep)]
+
+    def z_copy(kind, d, p=0):
         g = flip(fs, d, n_fs)
-        return copy(w_source(kind, g), w_slot(kind, fs, rep), z_send.at[kind, d - 1], z_recv.at[kind, d - 1], fs=g)
-
-    def y_copy(kind, d, e):
-        slot = w_slot(kind, flip(fs, d, n_fs), rep)
-        return copy(slot, slot, y_send.at[kind, d - 1, e - 1], y_recv.at[kind, d - 1, e - 1],
+        return copy(w_source(kind, g, p), w_slot(kind, fs, rep, p), z_send.at[kind + p, d - 1],
+                    z_recv.at[kind + p, d - 1], fs=g)
+
+    def y_copy(kind, d, e, p=0):
+        slot = w_slot(kind, flip(fs, d, n_fs), rep, p)
+        return copy(slot, slot, y_send.at[kind + p, d - 1, e - 1], y_recv.at[kind + p, d - 1, e - 1],
                     rep=lax.rem(rep + e, jnp.int32(n_rep)))
 
     def z_start(kind):
-        loop(1, n_fs, lambda d: z_copy(kind, d).start())
-
-    def y_relay(kind, d):
-        slot = w_slot(kind, flip(fs, d, n_fs), rep)
-        copy(slot, slot, z_send.at[kind, d - 1], z_recv.at[kind, d - 1], fs=pair).wait_recv()
+        def body(d):
+            for p in range(pieces if kind == DN else 1):
+                z_copy(kind, d, p).start()
+
+        loop(1, n_fs, body)
+
+    def y_relay(kind, d, p=0):
+        slot = w_slot(kind, flip(fs, d, n_fs), rep, p)
+        copy(slot, slot, z_send.at[kind + p, d - 1], z_recv.at[kind + p, d - 1], fs=pair).wait_recv()
         for e in range(1, n_rep):
-            y_copy(kind, d, e).start()
-
-    def y_ready(kind, d):
+            y_copy(kind, d, e, p).start()
+
+    def y_ready(kind, d, p=0):
         for e in range(1, n_rep):
-            slot = w_slot(kind, flip(fs, d, n_fs), lax.rem(rep - e + n_rep, jnp.int32(n_rep)))
-            copy(slot, slot, y_send.at[kind, d - 1, e - 1], y_recv.at[kind, d - 1, e - 1],
+            slot = w_slot(kind, flip(fs, d, n_fs), lax.rem(rep - e + n_rep, jnp.int32(n_rep)), p)
+            copy(slot, slot, y_send.at[kind + p, d - 1, e - 1], y_recv.at[kind + p, d - 1, e - 1],
                  rep=lax.rem(rep + 1, jnp.int32(n_rep))).wait_recv()
 
     def e_slot(kind, i, t):
@@ -224,15 +232,20 @@
         slot = resid_all.at[which, tp, rows_at(i, span)]
         return copy(slot, slot, p_send.at[i], p_recv.at[i], fs=pair)
 
-    def o_copy(d):
-        g = flip(fs, d, n_fs)
-        return copy(out_own, out_all.at[tp, owner_sub], o_send.at[d], o_recv.at[tp, owner_sub], fs=g, tp=owner)
+    def o_copy(k, sub):
+        to = lax.rem(tp + k, jnp.int32(n_tp))
+        return copy(out_gather.at[to * per_own + sub], out_all.at[tp, sub], o_send.at[k - 1, sub],
+                    o_recv.at[k - 1, sub], tp=to)
+
+    def o_take(k, sub):
+        sender = lax.rem(tp - k + n_tp, jnp.int32(n_tp))
+        copy(out_gather.at[0], out_all.at[sender, sub], o_send.at[k - 1, sub], o_recv.at[k - 1, sub],
+             tp=mate).wait_recv()
 
     def o_each(action):
-        def body(d):
-            on(jnp.logical_or(d > 0, owner != tp), lambda: action(d))
-
-        loop(0, n_fs, body)
+        for k in range(1, n_tp):
+            for sub in range(per_own):
+                action(k, sub)
 
     def s_copy(d, which):
         g = flip(fs, d, n_fs)
@@ -253,19 +266,12 @@
     def greet(**device):
         pl.semaphore_signal(barrier, inc=1, device_id=device, device_id_type=MESH)
 
-    greet(tp=mate)
-    for dx in range(1, n_x):
-        greet(tp=x_peer(dx))
+    for k in range(1, n_tp):
+        greet(tp=lax.rem(tp + k, jnp.int32(n_tp)))
     loop(1, n_fs, lambda d: greet(fs=flip(fs, d, n_fs)))
     for e in range(1, n_rep):
         greet(rep=lax.rem(rep + e, jnp.int32(n_rep)))
-
-    def greet_source(i):
-        f, t = tp * per_own + lax.div(i, jnp.int32(n_tp)), lax.rem(i, jnp.int32(n_tp))
-        on(jnp.logical_or(f != fs, t != tp), lambda: greet(fs=f, tp=t))
-
-    loop(0, per_own * n_tp, greet_source)
-    pl.semaphore_wait(barrier, 1 + (n_x - 1) + (n_fs - 1) + (n_rep - 1) + jnp.where(owner == tp, n_fs - 1, n_fs))
+    pl.semaphore_wait(barrier, n_tp + n_fs + n_rep - 3)
 
     loads[0].wait()
     loop(0, spans, lambda i: e_push(TOK, i))
@@ -275,15 +281,14 @@
     uv_all[fs, :, channels:2 * channels] = v_f[...].astype(jnp.bfloat16)
     z_start(UV)
     loads[3].wait()
-    out_own[...] = out_f[...].astype(jnp.bfloat16)
+    out_gather[fs] = out_f[...].astype(jnp.bfloat16)
+    z_start(OUT)
 
     def keep_own():
-        out_all[tp, owner_sub] = out_f[...].astype(jnp.bfloat16)
         scale_all[0, owner_sub] = out_scale_ref[...]
         scale_all[1, owner_sub] = down_scale_ref[...]
 
     on(owner == tp, keep_own)
-    o_each(lambda d: o_copy(d).start())
 
     def s_each(action):
         def body(d):
@@ -321,16 +326,19 @@
 
     def cast_down(i):
         here = rows_at(i, unit)
-        down_own[0, here] = down_f[here].astype(jnp.bfloat16)
-        there = jnp.where(i < main // unit, i + (main + LANES) // unit, main // unit + 1)
-        down_own[1, here] = down_f[rows_at(there, unit)].astype(jnp.bfloat16)
+        there = rows_at(jnp.where(i < main // unit, i + (main + LANES) // unit, main // unit + 1), unit)
+        for p in range(pieces):
+            cols = slice(p * width_down, (p + 1) * width_down)
+            down_own[0, p, here] = down_f[here, cols].astype(jnp.bfloat16)
+            down_own[1, p, here] = down_f[there, cols].astype(jnp.bfloat16)
 
     loop(0, hid // unit, cast_down)
-    keep_down = pltpu.make_async_copy(down_own.at[member], down_all.at[fs], local_sem.at[8])
+    keep_down = pltpu.make_async_copy(down_own.at[member], down_all.at[pl.ds(fs * pieces, pieces)], local_sem.at[8])
     keep_down.start()
 
     loop(0, spans, lambda i: e_relay(TOK, i))
     loop(1, n_fs, lambda d: y_relay(UV, d))
+    loop(1, n_fs, lambda d: y_relay(OUT, d))
     loop(1, n_fs, lambda d: y_ready(UV, d))
 
     eye = lax.broadcasted_iota(jnp.int32, (span, span), 0) == lax.broadcasted_iota(jnp.int32, (span, span), 1)
@@ -376,14 +384,13 @@
         e_push(GATED, i)
 
     loop(0, spans, mixer_span)
+    loop(1, n_fs, lambda d: y_ready(OUT, d))
+    o_each(lambda k, sub: o_copy(k, sub).start())
+    for sub in range(per_own):
+        out_all[tp, sub] = out_gather[tp * per_own + sub]
     loop(0, spans, lambda i: e_relay(GATED, i))
 
-    def out_arrived(i):
-        sub, t = lax.div(i, jnp.int32(n_tp)), lax.rem(i, jnp.int32(n_tp))
-        on(jnp.logical_or(tp * per_own + sub != fs, t != tp),
-           lambda: copy(out_own, out_all.at[t, sub], o_send.at[0], o_recv.at[t, sub], fs=pair, tp=mate).wait_recv())
-
-    loop(0, per_own * n_tp, out_arrived)
+    o_each(o_take)
 
     def scale_arrived(sub):
         def take():
@@ -411,8 +418,8 @@
         p_copy(i, member).start()
 
     loop(0, spans, resid_span)
-    for kind in (GU1, DN0, DN1):
-        z_start(kind)
+    z_start(GU1)
+    z_start(DN)
 
     def norm_span(which, i):
         here = rows_at(i, span)
@@ -457,7 +464,6 @@
         gu_acc[here, :] = jnp.dot(normed[fs, here, :], gu_all[fs], preferred_element_type=jnp.float32)
 
     loop(0, chunks, first_gu)
-    loop(1, n_fs, lambda d: y_relay(GU1, d))
 
     def fold_gu(d):
         y_ready(GU0, d)
@@ -470,23 +476,25 @@
 
         loop(0, chunks, body)
 
-    loop(1, n_fs, fold_gu)
+    def gu_step(d):
+        on(d < n_fs, lambda: y_relay(GU1, d))
+        on(d > 1, lambda: fold_gu(d - 1))
+
+    loop(1, n_fs + 1, gu_step)
 
     second = member == 1
-
-    def main_scale(ref):
-        return jnp.where(second, ref[:, main + LANES:], ref[:, 0:main])
-
-    gate_main, up_main = main_scale(gate_scale_ref), main_scale(up_scale_ref)
-    gs, us = gate_scale_ref[:, main:main + LANES], up_scale_ref[:, main:main + LANES]
-    last_scale = jnp.where(second, jnp.where(low, swap(gs), us), jnp.where(low, gs, swap(us)))
 
     def hidden_chunk(i):
         here = rows_at(i, 64)
-        a = gu_acc[here, 0:main] * gate_main
-        b = gu_acc[here, main:2 * main] * up_main
-        hidden[here, 0:main] = (a / (1.0 + jnp.exp(-a)) * b).astype(jnp.bfloat16)
-        a = gu_acc[here, 2 * main:] * last_scale
+        tiles = main // LANES
+        for j in range(tiles):
+            gate_scale = jnp.where(second, gate_scale_ref[tiles + 1 + j:tiles + 2 + j], gate_scale_ref[j:j + 1])
+            up_scale = jnp.where(second, up_scale_ref[tiles + 1 + j:tiles + 2 + j], up_scale_ref[j:j + 1])
+            a = gu_acc[here, j * LANES:(j + 1) * LANES] * gate_scale
+            b = gu_acc[here, main + j * LANES:main + (j + 1) * LANES] * up_scale
+            hidden[here, j * LANES:(j + 1) * LANES] = (a / (1.0 + jnp.exp(-a)) * b).astype(jnp.bfloat16)
+        gs, us = gate_scale_ref[tiles:tiles + 1], up_scale_ref[tiles:tiles + 1]
+        a = gu_acc[here, 2 * main:] * jnp.where(second, jnp.where(low, swap(gs), us), jnp.where(low, gs, swap(us)))
         b = swap(a)
         last = (a / (1.0 + jnp.exp(-a)) * b).astype(jnp.bfloat16)
         hidden[here, main:hid] = last[:, 0:hid - main]
@@ -494,13 +502,12 @@
     loop(0, total_rows // 64, hidden_chunk)
     keep_down.wait()
 
-    def block_at(k):
-        return fs - member + 0 if k is None else flip(fs - member, k, n_fs)
-
-    def places(k):
-        b = block_at(k)
+    def places(s):
+        d, p = lax.div(s, jnp.int32(pieces)), lax.rem(s, jnp.int32(pieces))
+        b = flip(fs, d, n_fs)
         own = lax.div(b, jnp.int32(per_own))
-        return b, lax.rem(own, two), lax.div(own, two), lax.rem(b, jnp.int32(per_own)), own
+        sub = lax.rem(b, jnp.int32(per_own)) * pieces + p
+        return b * pieces + p, lax.rem(own, two), lax.div(own, two), sub, own
 
     def m_copy(k, j):
         b, oc, ox, sub, own = places(k)
@@ -520,13 +527,8 @@
 
     def down_one(k):
         b, oc, ox, sub, own = places(k)
-        d = flip(member, k, n_fs)
-
-        def ready():
-            y_ready(DN0, d)
-            y_ready(DN1, d)
-
-        on(d > 0, ready)
+        d, p = lax.div(k, jnp.int32(pieces)), lax.rem(k, jnp.int32(pieces))
+        on(d > 0, lambda: y_ready(DN, d, p))
 
         def body(j):
             here = rows_at(j, CHUNK)
@@ -565,42 +567,38 @@
         on(own == tp, lambda: loop(0, chunks, body))
 
     def relay_down(k):
-        d = flip(member, k, n_fs)
-
-        def go():
-            y_relay(DN0, d)
-            y_relay(DN1, d)
-
-        on(d > 0, go)
+        d, p = lax.div(k, jnp.int32(pieces)), lax.rem(k, jnp.int32(pieces))
+        on(d > 0, lambda: y_relay(DN, d, p))
 
     def down_step(step):
-        on(step < n_fs, lambda: relay_down(step))
-        on(jnp.logical_and(step >= 1, step < n_fs + 1), lambda: down_one(step - 1))
-        on(jnp.logical_and(step >= 2, step < n_fs + 2), lambda: across(step - 2))
+        on(step < units, lambda: relay_down(step))
+        on(jnp.logical_and(step >= 1, step < units + 1), lambda: down_one(step - 1))
+        on(jnp.logical_and(step >= 2, step < units + 2), lambda: across(step - 2))
         on(step >= 3, lambda: collect(step - 3))
 
-    loop(0, n_fs + 3, down_step)
-
-    for sub in range(per_own):
-        b = tp * per_own + sub
-        cols = slice(sub * block, (sub + 1) * block)
+    loop(0, units + 3, down_step)
+
+    for sub in range(per_owner):
+        b = tp * per_owner + sub
+        cols = slice(sub * width_down, (sub + 1) * width_down)
 
         def close(j, b=b, sub=sub, cols=cols):
             here = rows_at(j, CHUNK)
             copy(part.at[b, here], pair_in.at[sub, here], q_send.at[sub, j], q_recv.at[sub, j], fs=pair).wait_recv()
             mine = rows_at(member * half_chunks + j, CHUNK)
             total = part[b, mine, :].astype(jnp.float32) + pair_in[sub, here, :].astype(jnp.float32)
-            total = (total * scale_all[1, sub]).astype(jnp.bfloat16).astype(jnp.float32)
+            total = (total * scale_all[1, sub // pieces, :, sub % pieces * width_down:(sub % pieces + 1) * width_down]).astype(jnp.bfloat16).astype(jnp.float32)
             kept = resid_all[member, tp, here, cols].astype(jnp.float32)
             result_ref[here, cols] = (kept + total).astype(jnp.bfloat16)
 
         loop(0, half_chunks, close)
 
-    for kind in range(KINDS):
+    for kind in range(5):
         def sent(d, kind=kind):
-            z_copy(kind, d).wait_send()
-            for e in range(1, n_rep):
-                y_copy(kind, d, e).wait_send()
+            for p in range(pieces if kind == DN else 1):
+                z_copy(kind, d, p).wait_send()
+                for e in range(1, n_rep):
+                    y_copy(kind, d, e, p).wait_send()
 
         loop(1, n_fs, sent)
 
@@ -610,7 +608,7 @@
         p_copy(i, member).wait_send()
 
     loop(0, spans, spans_sent)
-    o_each(lambda d: o_copy(d).wait_send())
+    o_each(lambda k, sub: o_copy(k, sub).wait_send())
     s_each(lambda c: c.wait_send())
 
     def parts_sent(k):
@@ -623,7 +621,7 @@
 
         loop(0, chunks, body)
 
-    loop(0, n_fs, parts_sent)
+    loop(0, units, parts_sent)
 
 
 def shards(
@@ -661,11 +659,13 @@
     per_own = own_width // block
     spans = rows // span_weight.shape[1]
     chunks = 2 * rows // CHUNK
+    pieces = max(block // (2 * LANES), 1)
+    width_down, per_owner, units = block // pieces, per_own * pieces, n_fs * pieces
     row = lambda vector: vector.reshape(1, -1)
     operands = (
         tokens, u_weight, v_weight, out_weight, gate_weight, up_weight, down_weight, row(out_scale), row(down_scale),
         row(pre_gain), row(ffn_gain), row(u_scale), row(v_scale), row(group_gain), span_weight, span_bias,
-        row(gate_scale), row(up_scale),
+        gate_scale.reshape(-1, LANES), up_scale.reshape(-1, LANES),
     )
     hbm, vmem = pl.BlockSpec(memory_space=pl.ANY), pl.BlockSpec(memory_space=pltpu.VMEM)
     bf16, f32 = jnp.bfloat16, jnp.float32
@@ -682,43 +682,43 @@
             pltpu.VMEM((block, local_hidden), f32),
             pltpu.VMEM((block, local_hidden), f32),
             pltpu.VMEM((local_hidden, block), f32),
-            pltpu.VMEM((channels, block), bf16),
             pltpu.VMEM((2, block, 2 * hid), bf16),
-            pltpu.VMEM((2, hid, block), bf16),
+            pltpu.VMEM((2, pieces, hid, width_down), bf16),
             pltpu.VMEM((n_tp, rows, own_width), bf16),
             pltpu.VMEM((n_fs, block, 2 * channels), bf16),
+            pltpu.VMEM((n_fs, channels, block), bf16),
             pltpu.VMEM((n_tp, per_own, channels, block), bf16),
             pltpu.VMEM((2, per_own, 1, block), f32),
             pltpu.VMEM((n_tp, rows, channels), bf16),
             pltpu.VMEM((2, n_tp, rows, own_width), bf16),
             pltpu.VMEM((n_fs, 2 * rows, block), bf16),
             pltpu.VMEM((n_fs, block, 2 * hid), bf16),
-            pltpu.VMEM((n_fs, hid, block), bf16),
+            pltpu.VMEM((units, hid, width_down), bf16),
             pltpu.VMEM((2 * rows, 2 * hid), f32),
             pltpu.VMEM((2 * rows, hid), bf16),
-            pltpu.VMEM((n_fs, 2 * rows, block), bf16),
-            pltpu.VMEM((n_x, per_own, 2 * rows, block), bf16),
-            pltpu.VMEM((n_x - 1, per_own, 2 * rows, block), bf16),
-            pltpu.VMEM((per_own, rows, block), bf16),
+            pltpu.VMEM((units, 2 * rows, width_down), bf16),
+            pltpu.VMEM((n_x, per_owner, 2 * rows, width_down), bf16),
+            pltpu.VMEM((n_x - 1, per_owner, 2 * rows, width_down), bf16),
+            pltpu.VMEM((per_owner, rows, width_down), bf16),
             dma(9),
-            dma(KINDS, n_fs - 1),
-            dma(KINDS, n_fs - 1),
-            dma(KINDS, n_fs - 1, n_rep - 1),
-            dma(KINDS, n_fs - 1, n_rep - 1),
+            dma(DN + pieces, n_fs - 1),
+            dma(DN + pieces, n_fs - 1),
+            dma(DN + pieces, n_fs - 1, n_rep - 1),
+            dma(DN + pieces, n_fs - 1, n_rep - 1),
             dma(4, spans, n_tp - 1),
             dma(4, spans, n_tp),
             dma(spans),
             dma(spans),
-            dma(n_fs),
-            dma(n_tp, per_own),
+            dma(n_tp - 1, per_own),
+            dma(n_tp - 1, per_own),
             dma(2, n_fs - 1),
             dma(2, per_own),
-            dma(n_fs, chunks),
-            dma(n_x, per_own, chunks),
-            dma(n_fs, chunks),
-            dma(n_x - 1, per_own, chunks),
-            dma(per_own, chunks // 2),
-            dma(per_own, chunks // 2),
+            dma(units, chunks),
+            dma(n_x, per_owner, chunks),
+            dma(units, chunks),
+            dma(n_x - 1, per_owner, chunks),
+            dma(per_owner, chunks // 2),
+            dma(per_owner, chunks // 2),
         ],
         compiler_params=pltpu.CompilerParams(
             collective_id=0, has_side_effects=True, vmem_limit_bytes=63 * 1024 * 1024

time: 195 us -> 178 us (0.913); the launches traced: 195 us -> 175 us
  Pallas kernels: 191 us -> 173 us
  local copies, waits for them, and re-layouts: 4.45 us -> 1.87 us
    pallas_call x1, Pallas kernels: 191 us -> 173 us  [shards(): pl.pallas_call(functools.partial(layer_kernel, sizes), out_shape=jax.Shap...]
    reshape x2 -> x0, local copies, waits for them, and re-layouts: 2.59 us -> none  [shards(): row = lambda vector: vector.reshape(1, -1)]
where the time goes in v2:
time: 178 us; the launch traced here: 175 us
  Pallas kernels  173 us (97%)
  local copies, waits for them, and re-layouts  1.87 us (1%)
    pallas_call x1, Pallas kernels, shards(): pl.pallas_call(functools.partial(layer_kernel, sizes), out_shape=jax.Shap...  173 us

profile of v2, /device:TPU:24, one launch (start us, length us, event | category | flops | bytes accessed | tf_op | source)
XLA Modules:
  0.0 174.9 jit_solution(16859763296937968651)
XLA Ops:
  0.0 173.1 %shard_map.172 = bf16[512,512]{1,0:T(8,128)(2,1)} custom-call(bf16[512,512]{1,0:T(8,128)(2,1)} %tokens_ref.1, f32[512,128]{1,0:T(8,128)} %u_ref.1, f32[512,128]{1,0:T(8,128)} %v_ref.1, f32[128,512]{1,0:T(8,128)} %out_ref.1, f32[512,1408]{1,0:T(8,128)} %gate_ref.1, f32[512,1408]{1,0:T(8,128)} %up_ref.1, f32[1408,512]{1,0:T(8,128)} %down_ref.1, ...), custom_call_target="tpu_custom_call" | custom-call | tf_op jit(solution)/shard_map/pallas_call | solution.py:673
  173.1 1.9 %copy.20 = bf16[512,512]{1,0:T(8,128)(2,1)} copy(bf16[512,512]{1,0:T(8,128)(2,1)} %shard_map.172) | data formatting | bytes 1048576

commit v3 on v2

--- a/solution.py
+++ b/solution.py
@@ -10,7 +10,8 @@
 EPS = 0.02
 MESH = pl.DeviceIdType.MESH
 LANES = 128
-UV, OUT, GU0, GU1, DN = range(5)
+CUTS = 8
+UV, OUT, GU, DN = 0, 1, 2, 2 + CUTS
 TOK, GATED, OWN, PAIR = range(4)
 CHUNK = 256
 
@@ -110,6 +111,8 @@
     block = gate_ref.shape[0]
     per_own = own_width // block
     hid = gate_ref.shape[1] // 2
+    cuts = min(CUTS, block // n_rep // 16)
+    early_cuts = cuts // 2
     pieces, width_down = down_own.shape[1], down_own.shape[3]
     per_owner = per_own * pieces
     units = n_fs * pieces
@@ -136,10 +139,10 @@
     def rows_at(i, size):
         return pl.ds(pl.multiple_of(i * size, size), size)
 
-    def w_rows(kind, r):
-        if kind in (GU0, GU1):
-            size = block // n_rep // 2
-            return pl.ds(pl.multiple_of((2 * r + (kind - GU0)) * size, size), size)
+    def w_rows(kind, r, p=0):
+        if kind == GU:
+            size = block // n_rep // cuts
+            return pl.ds(pl.multiple_of((cuts * r + p) * size, size), size)
         size = (block if kind == UV else channels if kind == OUT else hid) // n_rep
         return pl.ds(pl.multiple_of(r * size, size), size)
 
@@ -147,14 +150,14 @@
         if kind == DN:
             return down_all.at[f * pieces + p, w_rows(kind, r)]
         ref = uv_all if kind == UV else out_gather if kind == OUT else gu_all
-        return ref.at[f, w_rows(kind, r)]
+        return ref.at[f, w_rows(kind, r, p)]
 
     def w_source(kind, g, p=0):
         if kind in (UV, OUT):
             return w_slot(kind, fs, rep)
         if kind == DN:
             return down_own.at[lax.rem(g, two), p, w_rows(kind, rep)]
-        return gu_own.at[lax.rem(g, two), w_rows(kind, rep)]
+        return gu_own.at[lax.rem(g, two), w_rows(kind, rep, p)]
 
     def z_copy(kind, d, p=0):
         g = flip(fs, d, n_fs)
@@ -166,12 +169,16 @@
         return copy(slot, slot, y_send.at[kind + p, d - 1, e - 1], y_recv.at[kind + p, d - 1, e - 1],
                     rep=lax.rem(rep + e, jnp.int32(n_rep)))
 
-    def z_start(kind):
+    def z_start(kind, low=0, high=1):
         def body(d):
-            for p in range(pieces if kind == DN else 1):
+            for p in range(low, high):
                 z_copy(kind, d, p).start()
 
         loop(1, n_fs, body)
+
+    def unit_at(k):
+        k = jnp.int32(k)
+        return lax.div(k, jnp.int32(pieces)), lax.rem(k, jnp.int32(pieces))
 
     def y_relay(kind, d, p=0):
         slot = w_slot(kind, flip(fs, d, n_fs), rep, p)
@@ -319,7 +326,8 @@
         gu_own[1, here, 2 * main:] = jnp.where(low, swap(g), u).astype(jnp.bfloat16)
 
     loop(0, block // unit, cast_gu)
-    z_start(GU0)
+    for p in range(early_cuts):
+        z_start(GU, p, p + 1)
     keep_gu = pltpu.make_async_copy(gu_own.at[member], gu_all.at[fs], local_sem.at[7])
     keep_gu.start()
     loads[6].wait()
@@ -336,8 +344,13 @@
     keep_down = pltpu.make_async_copy(down_own.at[member], down_all.at[pl.ds(fs * pieces, pieces)], local_sem.at[8])
     keep_down.start()
 
-    loop(0, spans, lambda i: e_relay(TOK, i))
-    loop(1, n_fs, lambda d: y_relay(UV, d))
+
+    def first_relays(i):
+        e_relay(TOK, i)
+        on(i + 1 < n_fs, lambda: y_relay(UV, i + 1))
+
+    loop(0, spans, first_relays)
+    loop(spans + 1, n_fs, lambda d: y_relay(UV, d))
     loop(1, n_fs, lambda d: y_relay(OUT, d))
     loop(1, n_fs, lambda d: y_ready(UV, d))
 
@@ -390,6 +403,11 @@
         out_all[tp, sub] = out_gather[tp * per_own + sub]
     loop(0, spans, lambda i: e_relay(GATED, i))
 
+    def relay_gu(p):
+        loop(1, n_fs, lambda d: y_relay(GU, d, p))
+
+    relay_gu(0)
+
     o_each(o_take)
 
     def scale_arrived(sub):
@@ -418,8 +436,8 @@
         p_copy(i, member).start()
 
     loop(0, spans, resid_span)
-    z_start(GU1)
-    z_start(DN)
+    for p in range(early_cuts, cuts):
+        z_start(GU, p, p + 1)
 
     def norm_span(which, i):
         here = rows_at(i, span)
@@ -435,21 +453,32 @@
             gain = ffn_gain_ref[:, f * block:(f + 1) * block]
             normed[f, there, :] = (wide * inverse * gain).astype(jnp.bfloat16)
 
-    loop(0, spans, lambda i: e_relay(OWN, i))
+    done = 1
+    for i in range(spans):
+        e_relay(OWN, i)
+        if i % 2 and done < early_cuts - 1:
+            relay_gu(done)
+            done += 1
 
     def own_span(i):
         e_finish(OWN, i)
         norm_span(member, i)
 
     loop(0, spans, own_span)
-    loop(1, n_fs, lambda d: y_relay(GU0, d))
+    for p in range(done, early_cuts):
+        relay_gu(p)
 
     def pair_span(i):
         p_copy(i, 1 - member).wait_recv()
         e_push(PAIR, i)
 
     loop(0, spans, pair_span)
+    late = max(cuts - 2, early_cuts)
+    for p in range(early_cuts, late):
+        relay_gu(p)
     loop(0, spans, lambda i: e_relay(PAIR, i))
+    for p in range(late, cuts - 1):
+        relay_gu(p)
 
     def other_span(i):
         e_finish(PAIR, i)
@@ -459,15 +488,18 @@
 
     keep_gu.wait()
 
+    loop(pieces, units, lambda k: z_copy(DN, *unit_at(k)).start())
+
     def first_gu(i):
         here = rows_at(i, CHUNK)
         gu_acc[here, :] = jnp.dot(normed[fs, here, :], gu_all[fs], preferred_element_type=jnp.float32)
 
     loop(0, chunks, first_gu)
 
+
     def fold_gu(d):
-        y_ready(GU0, d)
-        y_ready(GU1, d)
+        for p in range(cuts):
+            y_ready(GU, d, p)
         f = flip(fs, d, n_fs)
 
         def body(i):
@@ -476,11 +508,10 @@
 
         loop(0, chunks, body)
 
-    def gu_step(d):
-        on(d < n_fs, lambda: y_relay(GU1, d))
-        on(d > 1, lambda: fold_gu(d - 1))
-
-    loop(1, n_fs + 1, gu_step)
+    relay_gu(cuts - 1)
+    loop(1, n_fs - 1, fold_gu)
+    loop(pieces, pieces + 1, lambda k: y_relay(DN, *unit_at(k)))
+    fold_gu(jnp.int32(n_fs - 1))
 
     second = member == 1
 
@@ -501,9 +532,10 @@
 
     loop(0, total_rows // 64, hidden_chunk)
     keep_down.wait()
+    loop(pieces + 1, pieces + 2, lambda k: y_relay(DN, *unit_at(k)))
 
     def places(s):
-        d, p = lax.div(s, jnp.int32(pieces)), lax.rem(s, jnp.int32(pieces))
+        d, p = unit_at(s)
         b = flip(fs, d, n_fs)
         own = lax.div(b, jnp.int32(per_own))
         sub = lax.rem(b, jnp.int32(per_own)) * pieces + p
@@ -527,7 +559,7 @@
 
     def down_one(k):
         b, oc, ox, sub, own = places(k)
-        d, p = lax.div(k, jnp.int32(pieces)), lax.rem(k, jnp.int32(pieces))
+        d, p = unit_at(k)
         on(d > 0, lambda: y_ready(DN, d, p))
 
         def body(j):
@@ -566,17 +598,13 @@
 
         on(own == tp, lambda: loop(0, chunks, body))
 
-    def relay_down(k):
-        d, p = lax.div(k, jnp.int32(pieces)), lax.rem(k, jnp.int32(pieces))
-        on(d > 0, lambda: y_relay(DN, d, p))
-
     def down_step(step):
-        on(step < units, lambda: relay_down(step))
-        on(jnp.logical_and(step >= 1, step < units + 1), lambda: down_one(step - 1))
-        on(jnp.logical_and(step >= 2, step < units + 2), lambda: across(step - 2))
-        on(step >= 3, lambda: collect(step - 3))
-
-    loop(0, units + 3, down_step)
+        down_one(step)
+        across(step)
+        on(jnp.logical_and(step >= pieces - 1, step + 3 < units), lambda: y_relay(DN, *unit_at(step + 3)))
+
+    loop(0, units, down_step)
+    loop(0, units, collect)
 
     for sub in range(per_owner):
         b = tp * per_owner + sub
@@ -593,9 +621,9 @@
 
         loop(0, half_chunks, close)
 
-    for kind in range(5):
-        def sent(d, kind=kind):
-            for p in range(pieces if kind == DN else 1):
+    for kind, count in ((UV, 1), (OUT, 1), (GU, cuts), (DN, pieces)):
+        def sent(d, kind=kind, count=count):
+            for p in range(count):
                 z_copy(kind, d, p).wait_send()
                 for e in range(1, n_rep):
                     y_copy(kind, d, e, p).wait_send()

time: 178 us -> 148 us (0.83)
  the two profiles are of different devices: /device:TPU:24 before, /device:TPU:25 now
where the time goes in v3:
time: 148 us
  Pallas kernels  146 us (99%)
  local copies, waits for them, and re-layouts  1.87 us (1%)
    pallas_call x1, Pallas kernels, shards(): pl.pallas_call(functools.partial(layer_kernel, sizes), out_shape=jax.Shap...  146 us

profile of v3, /device:TPU:25, one launch (start us, length us, event | category | flops | bytes accessed | tf_op | source)
XLA Modules:
  0.0 147.8 jit_solution(5249619235856086052)
XLA Ops:
  0.0 145.9 %shard_map.172 = bf16[512,512]{1,0:T(8,128)(2,1)} custom-call(bf16[512,512]{1,0:T(8,128)(2,1)} %tokens_ref.1, f32[512,128]{1,0:T(8,128)} %u_ref.1, f32[512,128]{1,0:T(8,128)} %v_ref.1, f32[128,512]{1,0:T(8,128)} %out_ref.1, f32[512,1408]{1,0:T(8,128)} %gate_ref.1, f32[512,1408]{1,0:T(8,128)} %up_ref.1, f32[1408,512]{1,0:T(8,128)} %down_ref.1, ...), custom_call_target="tpu_custom_call" | custom-call | tf_op jit(solution)/shard_map/pallas_call | solution.py:701
  146.0 1.9 %copy.20 = bf16[512,512]{1,0:T(8,128)(2,1)} copy(bf16[512,512]{1,0:T(8,128)(2,1)} %shard_map.172) | data formatting | bytes 1048576

commit v4 on v3

--- a/solution.py
+++ b/solution.py
@@ -159,6 +159,10 @@
             return down_own.at[lax.rem(g, two), p, w_rows(kind, rep)]
         return gu_own.at[lax.rem(g, two), w_rows(kind, rep, p)]
 
+    def z_pass(kind):
+        slot = w_slot(kind, flip(fs, 2, n_fs), rep)
+        return copy(slot, slot, z_send.at[kind, 2], z_recv.at[kind, 2], fs=pair)
+
     def z_copy(kind, d, p=0):
         g = flip(fs, d, n_fs)
         return copy(w_source(kind, g, p), w_slot(kind, fs, rep, p), z_send.at[kind + p, d - 1],
@@ -172,7 +176,7 @@
     def z_start(kind, low=0, high=1):
         def body(d):
             for p in range(low, high):
-                z_copy(kind, d, p).start()
+                on(d != 3 if kind in (UV, OUT) else True, lambda: z_copy(kind, d, p).start())
 
         loop(1, n_fs, body)
 
@@ -183,6 +187,8 @@
     def y_relay(kind, d, p=0):
         slot = w_slot(kind, flip(fs, d, n_fs), rep, p)
         copy(slot, slot, z_send.at[kind + p, d - 1], z_recv.at[kind + p, d - 1], fs=pair).wait_recv()
+        if kind in (UV, OUT):
+            on(d == 2, lambda: z_pass(kind).start())
         for e in range(1, n_rep):
             y_copy(kind, d, e, p).start()
 
@@ -326,8 +332,7 @@
         gu_own[1, here, 2 * main:] = jnp.where(low, swap(g), u).astype(jnp.bfloat16)
 
     loop(0, block // unit, cast_gu)
-    for p in range(early_cuts):
-        z_start(GU, p, p + 1)
+    z_start(GU, 0, 1)
     keep_gu = pltpu.make_async_copy(gu_own.at[member], gu_all.at[fs], local_sem.at[7])
     keep_gu.start()
     loads[6].wait()
@@ -352,6 +357,8 @@
     loop(0, spans, first_relays)
     loop(spans + 1, n_fs, lambda d: y_relay(UV, d))
     loop(1, n_fs, lambda d: y_relay(OUT, d))
+    for p in range(1, early_cuts):
+        z_start(GU, p, p + 1)
     loop(1, n_fs, lambda d: y_ready(UV, d))
 
     eye = lax.broadcasted_iota(jnp.int32, (span, span), 0) == lax.broadcasted_iota(jnp.int32, (span, span), 1)
@@ -456,7 +463,7 @@
     done = 1
     for i in range(spans):
         e_relay(OWN, i)
-        if i % 2 and done < early_cuts - 1:
+        if done < early_cuts:
             relay_gu(done)
             done += 1
 
@@ -468,17 +475,28 @@
     for p in range(done, early_cuts):
         relay_gu(p)
 
+    outer = jnp.logical_or(fs == 0, fs == n_fs - 1)
+    late = max(cuts - 2, early_cuts)
+
+    def relay_some(low, high):
+        for p in range(early_cuts, late - 1):
+            loop(low, high, lambda d: y_relay(GU, d, p))
+
+    on(outer, lambda: relay_some(2, n_fs))
+
     def pair_span(i):
         p_copy(i, 1 - member).wait_recv()
         e_push(PAIR, i)
 
     loop(0, spans, pair_span)
-    late = max(cuts - 2, early_cuts)
-    for p in range(early_cuts, late):
-        relay_gu(p)
-    loop(0, spans, lambda i: e_relay(PAIR, i))
+    relay_some(1, jnp.where(outer, 2, n_fs))
+    for p in range(late - 1, late):
+        loop(2, n_fs, lambda d: y_relay(GU, d, p))
+        y_relay(GU, 1, p)
+    loop(0, spans // 2, lambda i: e_relay(PAIR, i))
     for p in range(late, cuts - 1):
         relay_gu(p)
+    loop(spans // 2, spans, lambda i: e_relay(PAIR, i))
 
     def other_span(i):
         e_finish(PAIR, i)
@@ -532,7 +550,7 @@
 
     loop(0, total_rows // 64, hidden_chunk)
     keep_down.wait()
-    loop(pieces + 1, pieces + 2, lambda k: y_relay(DN, *unit_at(k)))
+    loop(pieces + 1, 2 * pieces + 1, lambda k: y_relay(DN, *unit_at(k)))
 
     def places(s):
         d, p = unit_at(s)
@@ -601,7 +619,7 @@
     def down_step(step):
         down_one(step)
         across(step)
-        on(jnp.logical_and(step >= pieces - 1, step + 3 < units), lambda: y_relay(DN, *unit_at(step + 3)))
+        on(jnp.logical_and(step >= 2 * pieces - 1, step + 2 < units), lambda: y_relay(DN, *unit_at(step + 2)))
 
     loop(0, units, down_step)
     loop(0, units, collect)
@@ -624,7 +642,11 @@
     for kind, count in ((UV, 1), (OUT, 1), (GU, cuts), (DN, pieces)):
         def sent(d, kind=kind, count=count):
             for p in range(count):
-                z_copy(kind, d, p).wait_send()
+                if kind in (UV, OUT):
+                    on(d == 3, lambda: z_pass(kind).wait_send())
+                    on(d != 3, lambda: z_copy(kind, d, p).wait_send())
+                else:
+                    z_copy(kind, d, p).wait_send()
                 for e in range(1, n_rep):
                     y_copy(kind, d, e, p).wait_send()
 

time: 148 us -> 142 us (0.959)
  the two profiles are of different devices: /device:TPU:25 before, /device:TPU:24 now
where the time goes in v4:
time: 142 us; the launch traced here: 139 us
  Pallas kernels  137 us (96%)
  local copies, waits for them, and re-layouts  1.87 us (1%)
    pallas_call x1, Pallas kernels, shards(): pl.pallas_call(functools.partial(layer_kernel, sizes), out_shape=jax.Shap...  137 us

profile of v4, /device:TPU:24, one launch (start us, length us, event | category | flops | bytes accessed | tf_op | source)
XLA Modules:
  0.0 138.9 jit_solution(8530847283439690586)
XLA Ops:
  0.0 137.1 %shard_map.172 = bf16[512,512]{1,0:T(8,128)(2,1)} custom-call(bf16[512,512]{1,0:T(8,128)(2,1)} %tokens_ref.1, f32[512,128]{1,0:T(8,128)} %u_ref.1, f32[512,128]{1,0:T(8,128)} %v_ref.1, f32[128,512]{1,0:T(8,128)} %out_ref.1, f32[512,1408]{1,0:T(8,128)} %gate_ref.1, f32[512,1408]{1,0:T(8,128)} %up_ref.1, f32[1408,512]{1,0:T(8,128)} %down_ref.1, ...), custom_call_target="tpu_custom_call" | custom-call | tf_op jit(solution)/shard_map/pallas_call | solution.py:723
  137.1 1.9 %copy.20 = bf16[512,512]{1,0:T(8,128)(2,1)} copy(bf16[512,512]{1,0:T(8,128)(2,1)} %shard_map.172) | data formatting | bytes 1048576

commit v5 on v4

--- a/solution.py
+++ b/solution.py
@@ -478,21 +478,28 @@
     outer = jnp.logical_or(fs == 0, fs == n_fs - 1)
     late = max(cuts - 2, early_cuts)
 
-    def relay_some(low, high):
-        for p in range(early_cuts, late - 1):
-            loop(low, high, lambda d: y_relay(GU, d, p))
-
-    on(outer, lambda: relay_some(2, n_fs))
+    def relay_one(p, low, high):
+        loop(low, high, lambda d: y_relay(GU, d, p))
+
+    on(outer, lambda: relay_one(early_cuts, 2, 3))
 
     def pair_span(i):
         p_copy(i, 1 - member).wait_recv()
         e_push(PAIR, i)
 
     loop(0, spans, pair_span)
-    relay_some(1, jnp.where(outer, 2, n_fs))
-    for p in range(late - 1, late):
-        loop(2, n_fs, lambda d: y_relay(GU, d, p))
-        y_relay(GU, 1, p)
+
+    def outer_rest():
+        for p in range(early_cuts, late):
+            relay_one(p, 3 if p == early_cuts else 2, n_fs)
+            relay_one(p, 1, 2)
+
+    def inner_rest():
+        for p in range(early_cuts, late):
+            relay_one(p, 1, n_fs)
+
+    on(outer, outer_rest)
+    on(jnp.logical_not(outer), inner_rest)
     loop(0, spans // 2, lambda i: e_relay(PAIR, i))
     for p in range(late, cuts - 1):
         relay_gu(p)
@@ -508,6 +515,8 @@
 
     loop(pieces, units, lambda k: z_copy(DN, *unit_at(k)).start())
 
+    relay_gu(cuts - 1)
+
     def first_gu(i):
         here = rows_at(i, CHUNK)
         gu_acc[here, :] = jnp.dot(normed[fs, here, :], gu_all[fs], preferred_element_type=jnp.float32)
@@ -526,7 +535,6 @@
 
         loop(0, chunks, body)
 
-    relay_gu(cuts - 1)
     loop(1, n_fs - 1, fold_gu)
     loop(pieces, pieces + 1, lambda k: y_relay(DN, *unit_at(k)))
     fold_gu(jnp.int32(n_fs - 1))
@@ -575,12 +583,16 @@
         src = part.at[b, rows_at((1 - member) * half_chunks + j, CHUNK)]
         return copy(src, pair_in.at[sub, rows_at(j, CHUNK)], q_send.at[sub, j], q_recv.at[sub, j], fs=pair)
 
+    def turned(i):
+        return lax.rem((1 - member) * half_chunks + i, jnp.int32(chunks))
+
     def down_one(k):
         b, oc, ox, sub, own = places(k)
         d, p = unit_at(k)
         on(d > 0, lambda: y_ready(DN, d, p))
 
-        def body(j):
+        def body(i):
+            j = turned(i)
             here = rows_at(j, CHUNK)
             part[b, here, :] = jnp.dot(hidden[here, :], down_all[b], preferred_element_type=jnp.float32).astype(
                 jnp.bfloat16)
@@ -591,7 +603,8 @@
     def across(k):
         b, oc, ox, sub, own = places(k)
 
-        def body(j):
+        def body(i):
+            j = turned(i)
             here = rows_at(j, CHUNK)
             m_copy(k, j).wait_recv()
             part[b, here, :] = (part[b, here, :].astype(jnp.float32)
@@ -604,7 +617,7 @@
         b, oc, ox, sub, own = places(k)
 
         def body(jj):
-            j = lax.rem((1 - member) * half_chunks + jj, jnp.int32(chunks))
+            j = turned(jj)
             here = rows_at(j, CHUNK)
             total = part[b, here, :].astype(jnp.float32)
             for dx in range(1, n_x):

time: 142 us -> 141 us (level)
  no operation moved by 1% of the time
where the time goes in v5:
time: 141 us; the launch traced here: 139 us
  Pallas kernels  137 us (97%)
  local copies, waits for them, and re-layouts  1.87 us (1%)
    pallas_call x1, Pallas kernels, shards(): pl.pallas_call(functools.partial(layer_kernel, sizes), out_shape=jax.Shap...  137 us

profile of v5, /device:TPU:24, one launch (start us, length us, event | category | flops | bytes accessed | tf_op | source)
XLA Modules:
  0.0 138.9 jit_solution(16592784664551687955)
XLA Ops:
  0.0 137.1 %shard_map.172 = bf16[512,512]{1,0:T(8,128)(2,1)} custom-call(bf16[512,512]{1,0:T(8,128)(2,1)} %tokens_ref.1, f32[512,128]{1,0:T(8,128)} %u_ref.1, f32[512,128]{1,0:T(8,128)} %v_ref.1, f32[128,512]{1,0:T(8,128)} %out_ref.1, f32[512,1408]{1,0:T(8,128)} %gate_ref.1, f32[512,1408]{1,0:T(8,128)} %up_ref.1, f32[1408,512]{1,0:T(8,128)} %down_ref.1, ...), custom_call_target="tpu_custom_call" | custom-call | tf_op jit(solution)/shard_map/pallas_call | solution.py:736
  137.1 1.9 %copy.20 = bf16[512,512]{1,0:T(8,128)(2,1)} copy(bf16[512,512]{1,0:T(8,128)(2,1)} %shard_map.172) | data formatting | bytes 1048576
